TPU v7x, 256 devices: a whole 4x4x8 slice. The times are simulated.
256 devices in a mesh: dp: 4 (over y), kv: 32 (over z, x), tp: 2 (over core).
Axes of the slice: x: 4, y: 4, z: 8, core: 2. Of those that a mesh axis runs over, the one named last changes fastest.
Arguments:
- tokens: bfloat16 [4, 24576, 2048], P('dp', 'kv'), may hold values from -60 to 60
- query_weight: bfloat16 [2048, 1024], P(None, 'tp'), may hold values from -0.125 to 0.125
- key_weight: bfloat16 [2048, 256], P(None, 'tp'), may hold values from -0.125 to 0.125
- value_weight: bfloat16 [2048, 256], P(None, 'tp'), may hold values from -0.125 to 0.125
- out_weight: bfloat16 [1024, 2048], P('tp'), may hold values from -3 to 3
- norm_gain: float32 [2048], P('tp'), may hold values from 0.1 to 1.9
- chosen_owner: int32 [4, 192, 16], P('dp'), may hold values from -1 to 31, as said below
- chosen_part: int32 [4, 192, 16], P('dp'), may hold values from 0 to 11, as said below
Outputs:
- attended: bfloat16 [4, 24576, 2048], P('dp', 'kv', 'tp')
Inputs may be any that keep to these rules, and one draw needn't show every extreme that they name: `chosen_owner`: within a row the indices other than -1 are different. Every named key block lies wholly before its query block's first position. Among the 6 rows of one index of kv, no index is named by more than 6 rows. `chosen_part`: 0 where the owner is -1.
All inputs are finite; a program needn't handle non-finite values.
Results may differ from a plain program's by a relative error of at most 0.014.
The roundings to bfloat16 on the way count: a program that leaves them out, or rounds other values in their place, can miss the bound.
Values may be sent and summed in bfloat16 or wider, within the bound.
A program may use at most 128 MiB of HBM per device.

v0:
```python
import jax
import jax.numpy as jnp
from jax import lax
from jax.sharding import PartitionSpec as P

D = 2048
HEAD_DIM = 64
QUERY_BLOCK = 128
KEY_BLOCK = 64


rope_base = 10000.0
norm_eps = 1e-06


def split_up(x, dim, count):
    before, after = (x.shape[:dim], x.shape[dim + 1 :])
    return jnp.moveaxis(x.reshape(*before, count, -1, *after), dim, 0)


def summed_on_arrival(x, axis, dim):
    count = lax.axis_size(axis)
    blocks = lax.all_to_all(split_up(x, dim, count), axis, 0, 0, tiled=True)
    return jnp.sum(blocks.astype(jnp.float32), axis=0)


def rotate(head_rows, positions):
    half_dim = head_rows.shape[-1] // 2
    frequency = rope_base ** (-jnp.arange(half_dim, dtype=jnp.float32) / half_dim)
    angles = positions.astype(jnp.float32)[:, None] * frequency
    cosine = jnp.cos(angles)[:, None, :]
    sine_part = jnp.sin(angles)[:, None, :]
    first_half = head_rows[..., :half_dim]
    second_half = head_rows[..., half_dim:]
    return jnp.concatenate(
        [
            first_half * cosine - second_half * sine_part,
            second_half * cosine + first_half * sine_part,
        ],
        axis=-1,
    )


def rank_within(flat_ids):
    entry_count = flat_ids.shape[0]
    same_owner = flat_ids[:, None] == flat_ids[None, :]
    earlier = jnp.arange(entry_count)[None, :] < jnp.arange(entry_count)[:, None]
    return jnp.sum(jnp.logical_and(same_owner, earlier), axis=1)


def body(
    tokens, query_weight, key_weight, value_weight, out_weight, norm_gain, chosen_owner, chosen_part
):
    row_data = tokens[0]
    tok_count = row_data.shape[0]
    devices = lax.axis_size("kv")
    my_index = lax.axis_index("kv")
    positions = my_index * tok_count + jnp.arange(tok_count, dtype=jnp.int32)
    heads_here = query_weight.shape[1] // HEAD_DIM
    kv_here = key_weight.shape[1] // HEAD_DIM
    group_size = heads_here // kv_here
    kv_width = kv_here * HEAD_DIM
    queries = rotate(
        jnp.dot(row_data, query_weight, preferred_element_type=jnp.float32).reshape(
            tok_count, heads_here, HEAD_DIM
        ),
        positions,
    ).astype(jnp.bfloat16)
    key_rows = (
        rotate(
            jnp.dot(row_data, key_weight, preferred_element_type=jnp.float32).reshape(
                tok_count, kv_here, HEAD_DIM
            ),
            positions,
        )
        .astype(jnp.bfloat16)
        .reshape(tok_count, kv_width)
    )
    value_rows = jnp.dot(row_data, value_weight, preferred_element_type=jnp.float32).astype(
        jnp.bfloat16
    )
    per_device = tok_count // KEY_BLOCK
    qblocks = tok_count // QUERY_BLOCK
    chosen_count = chosen_owner.shape[2]
    owner_ids = chosen_owner[0]
    part_ids = chosen_part[0]
    mine_owner = lax.dynamic_slice_in_dim(owner_ids, my_index * qblocks, qblocks, 0).reshape(
        qblocks * chosen_count
    )
    mine_valid = mine_owner >= 0
    key_blocks = key_rows.reshape(per_device, KEY_BLOCK, kv_width)
    value_blocks = value_rows.reshape(per_device, KEY_BLOCK, kv_width)
    every_owner = owner_ids.reshape(devices, qblocks * chosen_count)
    every_part = part_ids.reshape(devices, qblocks * chosen_count)
    every_rank = jax.vmap(rank_within)(every_owner)
    slot_ids = jnp.arange(qblocks, dtype=jnp.int32)
    picked_mask = jnp.logical_and(
        (every_owner == my_index)[:, None, :], every_rank[:, None, :] == slot_ids[None, :, None]
    )
    wanted = jnp.sum(jnp.where(picked_mask, every_part[:, None, :], 0), axis=2)
    send_keys = key_blocks[wanted]
    send_values = value_blocks[wanted]
    got_keys, got_values = (
        lax.all_to_all(send_keys, "kv", split_axis=0, concat_axis=0, tiled=True),
        lax.all_to_all(send_values, "kv", split_axis=0, concat_axis=0, tiled=True),
    )
    slot_index = jnp.where(mine_valid, mine_owner * qblocks + rank_within(mine_owner), 0)
    picked_keys = got_keys.reshape(devices * qblocks, KEY_BLOCK, kv_width)[slot_index]
    picked_values = got_values.reshape(devices * qblocks, KEY_BLOCK, kv_width)[slot_index]
    block_queries = queries.reshape(qblocks, QUERY_BLOCK, kv_here, group_size, HEAD_DIM)
    chosen_keys = picked_keys.reshape(qblocks, chosen_count * KEY_BLOCK, kv_here, HEAD_DIM)
    chosen_values = picked_values.reshape(qblocks, chosen_count * KEY_BLOCK, kv_here, HEAD_DIM)
    all_keys = jnp.concatenate(
        [chosen_keys, key_rows.reshape(qblocks, QUERY_BLOCK, kv_here, HEAD_DIM)], axis=1
    )
    all_values = jnp.concatenate(
        [chosen_values, value_rows.reshape(qblocks, QUERY_BLOCK, kv_here, HEAD_DIM)], axis=1
    )
    key_valid = jnp.broadcast_to(
        mine_valid.reshape(qblocks, chosen_count, 1), (qblocks, chosen_count, KEY_BLOCK)
    ).reshape(qblocks, chosen_count * KEY_BLOCK)
    far_mask = jnp.broadcast_to(
        key_valid[:, None, :], (qblocks, QUERY_BLOCK, chosen_count * KEY_BLOCK)
    )
    lower_mask = jnp.broadcast_to(
        (jnp.arange(QUERY_BLOCK)[:, None] >= jnp.arange(QUERY_BLOCK)[None, :])[None],
        (qblocks, QUERY_BLOCK, QUERY_BLOCK),
    )
    full_mask = jnp.concatenate([far_mask, lower_mask], axis=2)
    scores = jnp.einsum(
        "bqngd,bknd->bngqk", block_queries, all_keys, preferred_element_type=jnp.float32
    ) * HEAD_DIM ** (-0.5)
    scores = jnp.where(full_mask[:, None, None], scores, -jnp.inf)
    row_max = jnp.max(scores, axis=-1, keepdims=True)
    weights = jnp.exp(scores - row_max)
    weights = (weights / jnp.sum(weights, axis=-1, keepdims=True)).astype(jnp.bfloat16)
    mixed_rows = (
        jnp.einsum("bngqk,bknd->bqngd", weights, all_values, preferred_element_type=jnp.float32)
        .astype(jnp.bfloat16)
        .reshape(tok_count, heads_here * HEAD_DIM)
    )
    terms = jnp.dot(mixed_rows, out_weight, preferred_element_type=jnp.float32)
    projected = summed_on_arrival(terms.astype(jnp.bfloat16), "tp", 1)
    row_total = lax.psum(jnp.sum(projected * projected, axis=1), "tp")
    scale_rows = lax.rsqrt(row_total / D + norm_eps)
    result = (projected * scale_rows[:, None] * norm_gain[None, :]).astype(jnp.bfloat16)
    return result[None]


def solution(mesh):
    placed = (
        P("dp", "kv", None),
        P(None, "tp"),
        P(None, "tp"),
        P(None, "tp"),
        P("tp", None),
        P("tp"),
        P("dp", None, None),
        P("dp", None, None),
    )
    return jax.shard_map(
        body, mesh=mesh, in_specs=placed, out_specs=P("dp", "kv", "tp"), check_vma=False
    )
```

profile of v0, /device:TPU:1, one launch (start us, length us, event | category | flops | bytes accessed | tf_op | source)
XLA Modules:
  0.0 225.9 jit_solution(10290867702419029344)
XLA Ops:
  3.6 2.0 copy.58
  6.1 2.2 fusion.12
  11.4 2.8 %gather_fusion.2 = bf16[192,64,128]{2,1,0:T(8,128)(2,1)} fusion(bf16[12,64,128]{2,1,0:T(8,128)(2,1)S(1)} %convert_element_type.54, s32[1024]{0:T(1024)S(1)} %pad_clamp_fusion.1), kind=kCustom, calls=%fused_computation.2 | custom fusion | bytes 6292224 | tf_op jit(solution)/shard_map/gather | solution.py:101
  14.2 12.0 %all-to-all-start.1 = ((bf16[32,6,64,128]{3,2,1,0:T(8,128)(2,1)}), bf16[32,6,64,128]{3,2,1,0:T(8,128)(2,1)}, u32[]{:S(2)}, u32[]{:S(2)}) async-start(bf16[32,6,64,128]{3,2,1,0:T(8,128)(2,1)} %bitcast.110), calls=%async_computation.1 | async-start | bytes 6291456 | tf_op jit(solution)/shard_map/all_to_all | solution.py:104
  26.1 2.0 fusion.20
  28.2 2.8 %gather_fusion = bf16[192,64,128]{2,1,0:T(8,128)(2,1)} fusion(bf16[12,64,128]{2,1,0:T(8,128)(2,1)S(1)} %bitcast.108, s32[1024]{0:T(1024)S(1)} %pad_clamp_fusion.1), kind=kCustom, calls=%fused_computation | custom fusion | bytes 6292224 | tf_op jit(solution)/shard_map/gather | solution.py:102
  31.0 65.5 %all-to-all-done.1 = bf16[32,6,64,128]{3,2,1,0:T(8,128)(2,1)} async-done(((bf16[32,6,64,128]{3,2,1,0:T(8,128)(2,1)}), bf16[32,6,64,128]{3,2,1,0:T(8,128)(2,1)}, u32[]{:S(2)}, u32[]{:S(2)}) %all-to-all-start.1) | async-done | bytes 3145760 | tf_op jit(solution)/shard_map/all_to_all | solution.py:104
  96.5 8.2 %all-to-all-start = ((bf16[32,6,64,128]{3,2,1,0:T(8,128)(2,1)}), bf16[32,6,64,128]{3,2,1,0:T(8,128)(2,1)}, u32[]{:S(2)}, u32[]{:S(2)}) async-start(bf16[32,6,64,128]{3,2,1,0:T(8,128)(2,1)} %bitcast.109), calls=%async_computation | async-start | bytes 6291456 | tf_op jit(solution)/shard_map/all_to_all | solution.py:105
  109.1 3.9 %copy.63 = bf16[2048,512]{0,1:T(8,128)(2,1)} copy(bf16[2048,512]{1,0:T(8,128)(2,1)} %param.9) | data formatting | bytes 4194304 | tf_op args[1]
  113.1 3.4 %fusion.10 = f32[768,8,64]{0,2,1:T(8,128)S(1)} fusion(bf16[8,64,2048]{2,1,0:T(8,128)(2,1)} %bitcast.113, bf16[1,768,2048]{2,1,0:T(8,128)(2,1)S(1)} %copy-done), kind=kOutput, calls=%fused_computation.21 | convolution fusion | flops 1610612736 | bytes 6815744 | tf_op jit(solution)/shard_map/dot_general | solution.py:64
  121.7 3.8 %gather_fusion.3 = bf16[96,64,128]{2,1,0:T(8,128)(2,1)} fusion(bf16[192,64,128]{2,1,0:T(8,128)(2,1)} %bitcast.14, s32[1024]{0:T(1024)S(1)} %pad_clamp_fusion), kind=kCustom, calls=%fused_computation.3 | custom fusion | bytes 3146112 | tf_op jit(solution)/shard_map/gather | solution.py:108
  125.5 5.4 %reshape.262 = bf16[6,1024,2,64]{3,2,1,0:T(2,128)(2,1)S(1)} reshape(bf16[96,64,128]{2,1,0:T(8,128)(2,1)} %gather_fusion.3) | data formatting | bytes 3145728 | tf_op jit(solution)/shard_map/reshape | solution.py:111
  130.9 5.1 %copy.62 = bf16[6,1024,2,64]{1,3,2,0:T(8,128)(2,1)} copy(bf16[6,1024,2,64]{3,2,1,0:T(2,128)(2,1)S(1)} %reshape.262) | data formatting | bytes 3145728 | tf_op jit(solution)/shard_map/reshape | solution.py:111
  136.0 14.9 %fusion.23 = f32[6,2,1152,128,4]{3,2,4,1,0:T(8,128)} fusion(bf16[6,128,2,32]{1,3,2,0:T(8,128)(2,1)} %get-tuple-element.13, bf16[6,128,2,32]{1,3,2,0:T(8,128)(2,1)} %get-tuple-element.14, bf16[6,1024,2,64]{1,3,2,0:T(8,128)(2,1)} %copy.62, bf16[6,128,2,4,32]{1,4,3,2,0:T(8,128)(2,1)} %copy.65, bf16[6,128,2,4,32]{1,4,3,2,0:T(8,128)(2,1)S(1)} %copy.64), kind=kOutput, calls=%fused_computation.36 | convolution fusion | flops 912850944 | bytes 30867456 | tf_op jit(solution)/shard_map/bqngd,bknd->bngqk/dot_general | solution.py:130
  151.0 10.2 %fusion.39 = f32[6,2,4,128]{3,2,1,0:T(4,128)} fusion(pred[6,128,1152]{1,2,0:T(8,128)(4,1)S(1)} %copy-done.5, bf16[6,128,2,32]{1,3,2,0:T(8,128)(2,1)S(1)} %copy-done.11, bf16[6,128,2,32]{1,3,2,0:T(8,128)(2,1)S(1)} %copy-done.12, bf16[6,1024,2,64]{1,3,2,0:T(8,128)(2,1)S(1)} %copy-done.3, bf16[6,128,2,4,32]{1,4,3,2,0:T(8,128)(2,1)S(1)} %copy-done.4, ...), kind=kOutput, calls=%fused_computation.76 | convolution fusion | flops 941163648 | bytes 3465216 | tf_op jit(solution)/shard_map/sub | solution.py:135
  161.1 14.1 %all-to-all-done = bf16[32,6,64,128]{3,2,1,0:T(8,128)(2,1)} async-done(((bf16[32,6,64,128]{3,2,1,0:T(8,128)(2,1)}), bf16[32,6,64,128]{3,2,1,0:T(8,128)(2,1)}, u32[]{:S(2)}, u32[]{:S(2)}) %all-to-all-start) | async-done | bytes 3145760 | tf_op jit(solution)/shard_map/all_to_all | solution.py:105
  175.2 3.8 %gather_fusion.1 = bf16[96,64,128]{2,1,0:T(8,128)(2,1)} fusion(bf16[192,64,128]{2,1,0:T(8,128)(2,1)} %bitcast.4, s32[1024]{0:T(1024)S(1)} %pad_clamp_fusion), kind=kCustom, calls=%fused_computation.1 | custom fusion | bytes 3146112 | tf_op jit(solution)/shard_map/gather | solution.py:109
  179.1 5.4 %reshape.259 = bf16[6,1024,2,64]{3,2,1,0:T(2,128)(2,1)S(1)} reshape(bf16[96,64,128]{2,1,0:T(8,128)(2,1)} %gather_fusion.1) | data formatting | bytes 3145728 | tf_op jit(solution)/shard_map/reshape | solution.py:112
  184.4 5.1 %copy.56 = bf16[6,1024,2,64]{1,3,2,0:T(8,128)(2,1)} copy(bf16[6,1024,2,64]{3,2,1,0:T(2,128)(2,1)S(1)} %reshape.259) | data formatting | bytes 3145728 | tf_op jit(solution)/shard_map/reshape | solution.py:112
  189.6 14.9 %fusion.19 = bf16[6,128,2,4,64]{1,4,3,2,0:T(8,128)(2,1)S(1)} fusion(f32[6,2,4,128]{3,2,1,0:T(4,128)S(1)} %copy-done.16, f32[6,2,1152,128,4]{3,2,4,1,0:T(8,128)} %fusion.23, pred[6,128,1152]{1,2,0:T(8,128)(4,1)} %pad_add_fusion, bf16[6,128,2,64]{1,3,2,0:T(8,128)(2,1)S(1)} %copy-done.13, bf16[6,1024,2,64]{1,3,2,0:T(8,128)(2,1)} %copy.56), kind=kOutput, calls=%fused_computation.34 | convolution fusion | flops 945298560 | bytes 31776768 | tf_op jit(solution)/shard_map/bngqk,bknd->bqngd/dot_general | solution.py:138
  205.1 3.4 %convolution_convert_fusion = bf16[768,2048]{1,0:T(8,128)(2,1)S(1)} fusion(bf16[512,2048]{1,0:T(8,128)(2,1)} %param.12, bf16[64,8,6,128]{3,2,1,0:T(8,128)(2,1)S(1)} %bitcast.114), kind=kOutput, calls=%fused_computation.16 | convolution fusion | flops 1612185600 | bytes 6029312 | tf_op jit(solution)/shard_map/dot_general | solution.py:142
  208.9 8.4 %all_to_all.15 = bf16[2,768,1024]{2,1,0:T(8,128)(2,1)S(1)} all-to-all(bf16[2,768,1024]{2,1,0:T(8,128)(2,1)S(1)} %bitcast.111), channel_id=1, replica_groups=mesh['dp'=4,'kv'=32,'tp'=2] {'tp'}, dimensions={0} | all-to-all | bytes 6291456 | tf_op jit(solution)/shard_map/all_to_all | solution.py:23
  219.9 2.6 %psum.7 = f32[768]{0:T(1024)S(1)} all-reduce(f32[768]{0:T(1024)S(1)} %multiply_reduce_fusion), channel_id=1, replica_groups=mesh['dp'=4,'kv'=32,'tp'=2] {'tp'}, use_global_device_ids=true, to_apply=%region_7.8 | all-reduce | flops 768 | bytes 6144 | tf_op jit(solution)/shard_map/psum | solution.py:144
  222.6 3.4 %fusion.9 = bf16[1,768,1024]{2,1,0:T(8,128)(2,1)} fusion(f32[768,1024]{1,0:T(8,128)} %copy-done.2, f32[1024]{0:T(1024)S(1)} %copy-done.14, f32[768]{0:T(1024)S(1)} %add_rsqrt_fusion), kind=kLoop, calls=%fused_computation.20 | loop fusion | flops 2359296 | bytes 4725760 | tf_op jit(solution)/shard_map/convert_element_type | solution.py:146
  (81 shorter events, 20.1 us)
Async XLA Ops:
  0.0 6.1 %copy-start = (bf16[1,768,2048]{2,1,0:T(8,128)(2,1)S(1)}, bf16[1,768,2048]{2,1,0:T(8,128)(2,1)}, u32[]{:S(2)}) copy-start(bf16[1,768,2048]{2,1,0:T(8,128)(2,1)} %param.8) | copy-start | bytes 9437188
  1.0 7.3 %copy-start.10 = (s32[1,192,16]{2,1,0:T(8,128)}, s32[1,192,16]{2,1,0:T(8,128)S(1)}, u32[]{:S(2)}) copy-start(s32[1,192,16]{2,1,0:T(8,128)S(1)} %copy.51) | copy-start | bytes 36868
  8.4 0.6 copy-start.6
  8.4 0.7 copy-start.8
  14.2 82.3 %all-to-all-start.1 = ((bf16[32,6,64,128]{3,2,1,0:T(8,128)(2,1)}), bf16[32,6,64,128]{3,2,1,0:T(8,128)(2,1)}, u32[]{:S(2)}, u32[]{:S(2)}) async-start(bf16[32,6,64,128]{3,2,1,0:T(8,128)(2,1)} %bitcast.110), calls=%async_computation.1 | async-start | bytes 6291456 | tf_op jit(solution)/shard_map/all_to_all | solution.py:104
  96.5 78.8 %all-to-all-start = ((bf16[32,6,64,128]{3,2,1,0:T(8,128)(2,1)}), bf16[32,6,64,128]{3,2,1,0:T(8,128)(2,1)}, u32[]{:S(2)}, u32[]{:S(2)}) async-start(bf16[32,6,64,128]{3,2,1,0:T(8,128)(2,1)} %bitcast.109), calls=%async_computation | async-start | bytes 6291456 | tf_op jit(solution)/shard_map/all_to_all | solution.py:105
  116.5 2.2 copy-start.15
  116.5 2.3 %copy-start.7 = (bf16[768,2,32]{0,2,1:T(8,128)(2,1)S(1)}, bf16[768,2,32]{0,2,1:T(8,128)(2,1)}, u32[]{:S(2)}) copy-start(bf16[768,2,32]{0,2,1:T(8,128)(2,1)} %copy-done.6) | copy-start | bytes 294916
  116.5 2.3 %copy-start.9 = (bf16[768,2,32]{0,2,1:T(8,128)(2,1)S(1)}, bf16[768,2,32]{0,2,1:T(8,128)(2,1)}, u32[]{:S(2)}) copy-start(bf16[768,2,32]{0,2,1:T(8,128)(2,1)} %copy-done.8) | copy-start | bytes 294916
  136.0 15.0 %copy-start.3 = (bf16[6,1024,2,64]{1,3,2,0:T(8,128)(2,1)S(1)}, bf16[6,1024,2,64]{1,3,2,0:T(8,128)(2,1)}, u32[]{:S(2)}) copy-start(bf16[6,1024,2,64]{1,3,2,0:T(8,128)(2,1)} %copy.62) | copy-start | bytes 4718596
  136.0 15.0 %copy-start.4 = (bf16[6,128,2,4,32]{1,4,3,2,0:T(8,128)(2,1)S(1)}, bf16[6,128,2,4,32]{1,4,3,2,0:T(8,128)(2,1)}, u32[]{:S(2)}) copy-start(bf16[6,128,2,4,32]{1,4,3,2,0:T(8,128)(2,1)} %copy.65) | copy-start | bytes 1179652
  136.0 15.0 %copy-start.5 = (pred[6,128,1152]{1,2,0:T(8,128)(4,1)S(1)}, pred[6,128,1152]{1,2,0:T(8,128)(4,1)}, u32[]{:S(2)}) copy-start(pred[6,128,1152]{1,2,0:T(8,128)(4,1)} %pad_add_fusion) | copy-start | bytes 2654212
  136.0 15.0 %copy-start.11 = (bf16[6,128,2,32]{1,3,2,0:T(8,128)(2,1)S(1)}, bf16[6,128,2,32]{1,3,2,0:T(8,128)(2,1)}, u32[]{:S(2)}) copy-start(bf16[6,128,2,32]{1,3,2,0:T(8,128)(2,1)} %get-tuple-element.13) | copy-start | bytes 294916
  136.0 15.0 %copy-start.12 = (bf16[6,128,2,32]{1,3,2,0:T(8,128)(2,1)S(1)}, bf16[6,128,2,32]{1,3,2,0:T(8,128)(2,1)}, u32[]{:S(2)}) copy-start(bf16[6,128,2,32]{1,3,2,0:T(8,128)(2,1)} %get-tuple-element.14) | copy-start | bytes 294916
  184.4 5.2 %copy-start.13 = (bf16[6,128,2,64]{1,3,2,0:T(8,128)(2,1)S(1)}, bf16[6,128,2,64]{1,3,2,0:T(8,128)(2,1)}, u32[]{:S(2)}) copy-start(bf16[6,128,2,64]{1,3,2,0:T(8,128)(2,1)} %copy.57) | copy-start | bytes 589828
  184.4 5.2 %copy-start.16 = (f32[6,2,4,128]{3,2,1,0:T(4,128)S(1)}, f32[6,2,4,128]{3,2,1,0:T(4,128)}, u32[]{:S(2)}) copy-start(f32[6,2,4,128]{3,2,1,0:T(4,128)} %fusion.39) | copy-start | bytes 73732
  218.0 1.7 copy-start.2
  219.6 2.9 %copy-start.14 = (f32[1024]{0:T(1024)S(1)}, f32[1024]{0:T(1024)}, u32[]{:S(2)}) copy-start(f32[1024]{0:T(1024)} %param.13) | copy-start | bytes 12292
  219.7 6.3 %copy-start.1 = (bf16[1,768,2048]{2,1,0:T(8,128)(2,1)S(1)}, bf16[1,768,2048]{2,1,0:T(8,128)(2,1)}, u32[]{:S(2)}) copy-start(bf16[1,768,2048]{2,1,0:T(8,128)(2,1)} %param.8) | copy-start | bytes 9437188
where the time goes:
time: 227 us; the launch traced here: 226 us
  waiting for transfers between devices  79.6 us (35%)
  local copies, waits for them, and re-layouts  55.3 us (24%)
  matrix products  51.1 us (23%)
  starting transfers between devices  20.2 us (9%)
  blocking collectives  11 us (5%)
  other arithmetic  8.32 us (4%)
    all_to_all x1, waiting for transfers between devices, body(): lax.all_to_all(send_keys, 'kv', split_axis=0, concat_axis=0, tiled=True)  65.5 us
    dot_general x1, matrix products, body(): jnp.einsum('bqngd,bknd->bngqk', block_queries, all_keys, preferred_elemen...  14.9 us
    dot_general x1, matrix products, body(): jnp.einsum('bngqk,bknd->bqngd', weights, all_values, preferred_element_ty...  14.9 us
    all_to_all x1, waiting for transfers between devices, body(): lax.all_to_all(send_values, 'kv', split_axis=0, concat_axis=0, tiled=True)  14.1 us
    all_to_all x1, starting transfers between devices, body(): lax.all_to_all(send_keys, 'kv', split_axis=0, concat_axis=0, tiled=True)  12 us
    reshape x2, local copies, waits for them, and re-layouts, body(): picked_keys.reshape(qblocks, chosen_count * KEY_BLOCK, kv_here, HEAD_DIM)  10.5 us
    reshape x2, local copies, waits for them, and re-layouts, body(): picked_values.reshape(qblocks, chosen_count * KEY_BLOCK, kv_here, HEAD_DIM)  10.5 us
    sub x1, matrix products, body(): weights = jnp.exp(scores - row_max)  10.2 us
  transfers between devices with their start and end apart: 2, of which 2 were waited for; matrix products, arithmetic and copies ran while one was open for 27% of the time, Pallas kernels for 0%

commit v1 on v0

v1 whole, which is shorter than its diff:
```python
import jax
import jax.numpy as jnp
from jax import lax
from jax.experimental import pallas as pl
from jax.experimental.pallas import tpu as pltpu
from jax.sharding import PartitionSpec as P

D = 2048
HEAD_DIM = 64
QUERY_BLOCK = 128
KEY_BLOCK = 64
NZ = 8
NX = 4
ROWS = 6
PARTS = 12
CHOSEN = 16
FULL = NZ * PARTS
SEL = NZ * ROWS
BLOCKS = 2 * FULL + 2 * SEL
rope_base = 10000.0
norm_eps = 1e-06
MESH = pl.DeviceIdType.MESH
LOG2E = 1.4426950408889634


def split_up(x, dim, count):
    before, after = (x.shape[:dim], x.shape[dim + 1 :])
    return jnp.moveaxis(x.reshape(*before, count, -1, *after), dim, 0)


def summed_on_arrival(x, axis, dim):
    count = lax.axis_size(axis)
    blocks = lax.all_to_all(split_up(x, dim, count), axis, 0, 0, tiled=True)
    return jnp.sum(blocks.astype(jnp.float32), axis=0)


def turned(u, cosine, sine, low_half):
    other = jnp.where(low_half, pltpu.roll(u, 96, 1), pltpu.roll(u, 32, 1))
    return u * cosine + other * sine


def project_kernel(x_ref, wq_ref, wk_ref, wv_ref, cos_ref, sin_ref, q_ref, k_ref, v_ref):
    x = x_ref[...]
    cosine, sine = cos_ref[...], sin_ref[...]
    lane = lax.broadcasted_iota(jnp.int32, cosine.shape, 1)
    low_half = (lane % HEAD_DIM) < HEAD_DIM // 2
    first_head = lane < HEAD_DIM
    keys = jnp.dot(x, wk_ref[...], preferred_element_type=jnp.float32)
    k_ref[...] = turned(keys, cosine, sine, low_half).astype(jnp.bfloat16)
    v_ref[...] = jnp.dot(x, wv_ref[...], preferred_element_type=jnp.float32).astype(jnp.bfloat16)
    q = jnp.dot(x, wq_ref[...], preferred_element_type=jnp.float32)
    raw = [turned(q[:, 128 * i : 128 * (i + 1)], cosine, sine, low_half) for i in range(4)]
    swapped = [pltpu.roll(u, 64, 1) for u in raw]
    paired = [
        jnp.where(first_head, raw[0], swapped[2]),
        jnp.where(first_head, swapped[0], raw[2]),
        jnp.where(first_head, raw[1], swapped[3]),
        jnp.where(first_head, swapped[1], raw[3]),
    ]
    for i in range(4):
        q_ref[:, 128 * i : 128 * (i + 1)] = paired[i].astype(jnp.bfloat16)


def exchange_kernel(t_ref, k_ref, v_ref, kb_ref, vb_ref, whole, stage, zsend, zrecv, nsend, nrecv, ssend, srecv):
    me = lax.axis_index("kv")
    z, x = me // NX, me % NX
    up = ((z + 1) % NZ) * NX + x
    down = ((z + NZ - 1) % NZ) * NX + x
    right = z * NX + (x + 1) % NX
    left = z * NX + (x + NX - 1) % NX
    xr, xl = (x + 1) % NX, (x + NX - 1) % NX
    barrier = pltpu.get_barrier_semaphore()
    for peer in (up, down, right, left):
        pl.semaphore_signal(barrier, inc=1, device_id={"kv": peer}, device_id_type=MESH)
    pl.semaphore_wait(barrier, 4)
    sent = []

    def send(src, dst, ssem, rsem, peer):
        copy = pltpu.make_async_remote_copy(
            src_ref=src, dst_ref=dst, send_sem=ssem, recv_sem=rsem,
            device_id={"kv": peer}, device_id_type=MESH,
        )
        copy.start()
        sent.append(copy)
        return copy

    bufs = (kb_ref, vb_ref, kb_ref, vb_ref)
    bases = (0, 0, FULL, FULL)

    def chunk(kind, slot):
        return bufs[kind].at[pl.ds(bases[kind] + slot * PARTS, PARTS)]

    arrivals = {}

    def forward(kind, direction, step, src):
        slot = step if direction == 0 else NZ - step
        arrivals[direction, step, kind] = send(
            src, chunk(kind, slot), zsend.at[direction, step - 1, kind],
            zrecv.at[direction, step - 1, kind], up if direction == 0 else down,
        )

    def pick(kind, slot):
        buf = bufs[kind]
        owner_x = (x, x, xl, xr)[kind]
        dest_x, dest = ((xl, left), (xr, right), (xr, right), (xl, left))[kind]
        owner = ((z + NZ - slot) % NZ) * NX + owner_x
        base = bases[kind] + slot * PARTS
        whole[...] = buf[base : base + PARTS]
        for r in range(ROWS):
            part = t_ref[(dest_x * ROWS + r) * (NZ * NX) + owner]
            stage[slot, kind, r] = whole[part]
        place = 2 * FULL + (SEL if kind >= 2 else 0) + slot * ROWS
        return send(
            stage.at[slot, kind], buf.at[pl.ds(place, ROWS)],
            ssend.at[slot, kind], srecv.at[slot, kind], dest,
        )

    for direction in range(2):
        forward(0, direction, 1, k_ref)
        forward(1, direction, 1, v_ref)
    near = [
        send(k_ref, chunk(2, 0), nsend.at[0], nrecv.at[0], right),
        send(v_ref, chunk(3, 0), nsend.at[1], nrecv.at[1], left),
    ]
    kb_ref[0:PARTS] = k_ref[...]
    vb_ref[0:PARTS] = v_ref[...]
    picked = [pick(0, 0), pick(1, 0)]
    for kind in (2, 3):
        near[kind - 2].wait_recv()
        forward(kind, 0, 1, chunk(kind, 0))
        forward(kind, 1, 1, chunk(kind, 0))
        picked.append(pick(kind, 0))
    half = NZ // 2
    for step in range(1, half + 1):
        for kind in range(4):
            ready = []
            for direction in range(2):
                if (direction, step, kind) not in arrivals:
                    continue
                arrivals[direction, step, kind].wait_recv()
                slot = step if direction == 0 else NZ - step
                ready.append(slot)
                if step + 1 < half or (step + 1 == half and kind % 2 == direction):
                    forward(kind, direction, step + 1, chunk(kind, slot))
            for slot in ready:
                picked.append(pick(kind, slot))
    for copy in picked:
        copy.wait_recv()
    for copy in sent:
        copy.wait_send()


def attend_kernel(kidx_ref, vidx_ref, bias_ref, q_ref, k_ref, v_ref, kb_ref, vb_ref, out_ref, keys, values, ksem, vsem):
    b = pl.program_id(0)
    count = pl.num_programs(0)

    def fetch(row, slot, start):
        for s in range(CHOSEN):
            kcopy = pltpu.make_async_copy(
                kb_ref.at[kidx_ref[row * CHOSEN + s]],
                keys.at[slot, pl.ds(s * KEY_BLOCK, KEY_BLOCK)], ksem.at[slot, s])
            vcopy = pltpu.make_async_copy(
                vb_ref.at[vidx_ref[row * CHOSEN + s]],
                values.at[slot, pl.ds(s * KEY_BLOCK, KEY_BLOCK), pl.ds(0, 128)], vsem.at[slot, s])
            if start:
                kcopy.start()
                vcopy.start()
            else:
                kcopy.wait()
                vcopy.wait()

    @pl.when(b == 0)
    def _():
        fetch(0, 0, True)
        for slot in range(2):
            values[slot, :, 128:256] = jnp.ones((values.shape[1], 128), jnp.bfloat16)

    slot = lax.rem(b, 2)
    far = CHOSEN * KEY_BLOCK

    @pl.when(b + 1 < count)
    def _():
        fetch(b + 1, 1 - slot, True)

    fetch(b, slot, False)
    keys[slot, far:, :] = k_ref[...]
    values[slot, far:, 0:128] = v_ref[...]
    all_keys = keys[slot]
    all_values = values[slot]
    lane = lax.broadcasted_iota(jnp.int32, (QUERY_BLOCK, 128), 1)
    first_head = lane < HEAD_DIM
    query_at = lax.broadcasted_iota(jnp.int32, (QUERY_BLOCK, QUERY_BLOCK), 0)
    key_at = lax.broadcasted_iota(jnp.int32, (QUERY_BLOCK, QUERY_BLOCK), 1)
    causal = query_at >= key_at
    bias = bias_ref[0]
    scale = HEAD_DIM ** -0.5 * LOG2E
    mixed = []
    for g in range(4):
        q = q_ref[:, 128 * g : 128 * (g + 1)]
        parts = []
        for n in range(2):
            own = jnp.where(first_head if n == 0 else jnp.logical_not(first_head), q, jnp.zeros_like(q))
            scores = lax.dot_general(own, all_keys, (((1,), (1,)), ((), ())), preferred_element_type=jnp.float32)
            scores_far = scores[:, :far] + bias
            scores_own = jnp.where(causal, scores[:, far:], -jnp.inf)
            top = jnp.maximum(
                jnp.max(scores_far, axis=1, keepdims=True), jnp.max(scores_own, axis=1, keepdims=True))
            weights = jnp.concatenate(
                [jnp.exp2((scores_far - top) * scale).astype(jnp.bfloat16),
                 jnp.exp2((scores_own - top) * scale).astype(jnp.bfloat16)], axis=1)
            summed = jnp.dot(weights, all_values, preferred_element_type=jnp.float32)
            parts.append(summed[:, :128] / summed[:, 128:])
        mixed.append(jnp.where(first_head, parts[0], parts[1]))
    swapped = [pltpu.roll(u, 64, 1) for u in mixed]
    ordered = [
        jnp.where(first_head, mixed[0], swapped[1]),
        jnp.where(first_head, mixed[2], swapped[3]),
        jnp.where(first_head, swapped[0], mixed[1]),
        jnp.where(first_head, swapped[2], mixed[3]),
    ]
    for i in range(4):
        out_ref[:, 128 * i : 128 * (i + 1)] = ordered[i].astype(jnp.bfloat16)


def body(
    tokens, query_weight, key_weight, value_weight, out_weight, norm_gain, chosen_owner, chosen_part
):
    row_data = tokens[0]
    tok_count = row_data.shape[0]
    me = lax.axis_index("kv")
    z, x = me // NX, me % NX
    positions = me * tok_count + jnp.arange(tok_count, dtype=jnp.int32)
    half_dim = HEAD_DIM // 2
    frequency = rope_base ** (-jnp.arange(half_dim, dtype=jnp.float32) / half_dim)
    angles = positions.astype(jnp.float32)[:, None] * frequency
    cosine, sine = jnp.cos(angles), jnp.sin(angles)
    cosine = jnp.concatenate([cosine] * 4, axis=1)
    sine = jnp.concatenate([-sine, sine, -sine, sine], axis=1)
    tile = 256
    queries, keys, values = pl.pallas_call(
        project_kernel,
        grid=(tok_count // tile,),
        in_specs=[
            pl.BlockSpec((tile, D), lambda i: (i, 0)),
            pl.BlockSpec((D, 512), lambda i: (0, 0)),
            pl.BlockSpec((D, 128), lambda i: (0, 0)),
            pl.BlockSpec((D, 128), lambda i: (0, 0)),
            pl.BlockSpec((tile, 128), lambda i: (i, 0)),
            pl.BlockSpec((tile, 128), lambda i: (i, 0)),
        ],
        out_specs=[
            pl.BlockSpec((tile, 512), lambda i: (i, 0)),
            pl.BlockSpec((tile, 128), lambda i: (i, 0)),
            pl.BlockSpec((tile, 128), lambda i: (i, 0)),
        ],
        out_shape=[
            jax.ShapeDtypeStruct((tok_count, 512), jnp.bfloat16),
            jax.ShapeDtypeStruct((tok_count, 128), jnp.bfloat16),
            jax.ShapeDtypeStruct((tok_count, 128), jnp.bfloat16),
        ],
    )(row_data, query_weight, key_weight, value_weight, cosine, sine)

    owners, parts = chosen_owner[0], chosen_part[0]
    row_owner = lax.dynamic_slice_in_dim(owners, z * NX * ROWS, NX * ROWS, 0)
    row_part = lax.dynamic_slice_in_dim(parts, z * NX * ROWS, NX * ROWS, 0)
    everyone = jnp.arange(NZ * NX, dtype=jnp.int32)
    table = jnp.sum(
        jnp.where(row_owner[:, :, None] == everyone, row_part[:, :, None], 0), axis=1
    ).reshape(NX * ROWS * NZ * NX)
    mine_owner = lax.dynamic_slice_in_dim(owners, me * ROWS, ROWS, 0)
    mine_part = lax.dynamic_slice_in_dim(parts, me * ROWS, ROWS, 0)
    valid = mine_owner >= 0
    safe = jnp.maximum(mine_owner, 0)
    slot = (z - safe // NX + NZ) % NZ
    across = (safe % NX - x + NX) % NX
    row = jnp.arange(ROWS, dtype=jnp.int32)[:, None]
    full_at = slot * PARTS + mine_part
    sel_at = 2 * FULL + slot * ROWS + row
    kidx = jnp.where(across == 0, full_at, jnp.where(across == 3, FULL + full_at, jnp.where(across == 1, sel_at, SEL + sel_at)))
    vidx = jnp.where(across == 0, full_at, jnp.where(across == 1, FULL + full_at, jnp.where(across == 3, sel_at, SEL + sel_at)))
    kidx = jnp.where(valid, kidx, 0).reshape(ROWS * CHOSEN)
    vidx = jnp.where(valid, vidx, 0).reshape(ROWS * CHOSEN)
    bias = jnp.where(jnp.repeat(valid, KEY_BLOCK, axis=1), 0.0, -jnp.inf).astype(jnp.float32)[:, None, :]

    vmem = pl.BlockSpec(memory_space=pltpu.VMEM)
    smem = pl.BlockSpec(memory_space=pltpu.SMEM)
    anyspace = pl.BlockSpec(memory_space=pl.ANY)
    pool = jax.ShapeDtypeStruct((BLOCKS, KEY_BLOCK, 128), jnp.bfloat16)
    kb, vb = pl.pallas_call(
        exchange_kernel,
        in_specs=[smem, vmem, vmem],
        out_specs=[vmem, vmem],
        out_shape=[pool, pool],
        scratch_shapes=[
            pltpu.VMEM((PARTS, KEY_BLOCK, 128), jnp.bfloat16),
            pltpu.VMEM((NZ, 4, ROWS, KEY_BLOCK, 128), jnp.bfloat16),
            pltpu.SemaphoreType.DMA((2, NZ // 2, 4)),
            pltpu.SemaphoreType.DMA((2, NZ // 2, 4)),
            pltpu.SemaphoreType.DMA((2,)),
            pltpu.SemaphoreType.DMA((2,)),
            pltpu.SemaphoreType.DMA((NZ, 4)),
            pltpu.SemaphoreType.DMA((NZ, 4)),
        ],
        compiler_params=pltpu.CompilerParams(collective_id=0, has_side_effects=True),
    )(table, keys.reshape(PARTS, KEY_BLOCK, 128), values.reshape(PARTS, KEY_BLOCK, 128))

    mixed_rows = pl.pallas_call(
        attend_kernel,
        grid_spec=pltpu.PrefetchScalarGridSpec(
            num_scalar_prefetch=2,
            grid=(ROWS,),
            in_specs=[
                pl.BlockSpec((1, 1, CHOSEN * KEY_BLOCK), lambda i, a, c: (i, 0, 0)),
                pl.BlockSpec((QUERY_BLOCK, 512), lambda i, a, c: (i, 0)),
                pl.BlockSpec((QUERY_BLOCK, 128), lambda i, a, c: (i, 0)),
                pl.BlockSpec((QUERY_BLOCK, 128), lambda i, a, c: (i, 0)),
                anyspace,
                anyspace,
            ],
            out_specs=pl.BlockSpec((QUERY_BLOCK, 512), lambda i, a, c: (i, 0)),
            scratch_shapes=[
                pltpu.VMEM((2, CHOSEN * KEY_BLOCK + QUERY_BLOCK, 128), jnp.bfloat16),
                pltpu.VMEM((2, CHOSEN * KEY_BLOCK + QUERY_BLOCK, 256), jnp.bfloat16),
                pltpu.SemaphoreType.DMA((2, CHOSEN)),
                pltpu.SemaphoreType.DMA((2, CHOSEN)),
            ],
        ),
        out_shape=jax.ShapeDtypeStruct((tok_count, 512), jnp.bfloat16),
    )(kidx, vidx, bias, queries, keys, values, kb, vb)

    terms = jnp.dot(mixed_rows, out_weight, preferred_element_type=jnp.float32)
    projected = summed_on_arrival(terms.astype(jnp.bfloat16), "tp", 1)
    row_total = lax.psum(jnp.sum(projected * projected, axis=1), "tp")
    scale_rows = lax.rsqrt(row_total / D + norm_eps)
    result = (projected * scale_rows[:, None] * norm_gain[None, :]).astype(jnp.bfloat16)
    return result[None]


def solution(mesh):
    placed = (
        P("dp", "kv", None),
        P(None, "tp"),
        P(None, "tp"),
        P(None, "tp"),
        P("tp", None),
        P("tp"),
        P("dp", None, None),
        P("dp", None, None),
    )
    return jax.shard_map(
        body, mesh=mesh, in_specs=placed, out_specs=P("dp", "kv", "tp"), check_vma=False
    )
```

time: 227 us -> 131 us (0.58)
  Pallas kernels: 0 us -> 102 us
  waiting for transfers between devices: 79.6 us -> 0 us
  local copies, waits for them, and re-layouts: 55.3 us -> 6.04 us
  matrix products: 51.1 us -> 2.93 us
  starting transfers between devices: 20.2 us -> 0 us
    pallas_call x0 -> x3, Pallas kernels: none -> 102 us  [the longest x1 76.7 us: body(): pl.pallas_call(exchange_kernel, in_specs=[smem, vmem, vmem], out_specs=[v...]
    all_to_all x2 -> x0, waiting for transfers between devices: 79.6 us -> none  [the longest x1 65.5 us: body(): lax.all_to_all(send_keys, 'kv', split_axis=0, concat_axis=0, tiled=True)]
    dot_general x5 -> x0, matrix products: 37.5 us -> none  [the longest x1 14.9 us: body(): jnp.einsum('bqngd,bknd->bngqk', block_queries, all_keys, preferred_elemen...]
    reshape x6 -> x1, local copies, waits for them, and re-layouts: 23.8 us -> 0.66 us  [body(): table = jnp.sum(jnp.where(row_owner[:, :, None] == everyone, row_part[:,...]
    all_to_all x2 -> x0, starting transfers between devices: 20.2 us -> none  [the longest x1 12 us: body(): lax.all_to_all(send_keys, 'kv', split_axis=0, concat_axis=0, tiled=True)]
    gather x4 -> x0, local copies, waits for them, and re-layouts: 13.2 us -> none  [the longest x1 3.83 us: body(): got_values.reshape(devices * qblocks, KEY_BLOCK, kv_width)[slot_index]]
    sub x1 -> x0, matrix products: 10.2 us -> none  [body(): weights = jnp.exp(scores - row_max)]
    unnamed x38 -> x7, local copies, waits for them, and re-layouts: 10.1 us -> 1.74 us
  transfers between devices with their start and end apart: 2 -> 0, of which waited for: 2 -> 0; matrix products, arithmetic and copies ran while one was open for 27% -> 0% of each run, Pallas kernels for 0% -> 0%
where the time goes in v1:
time: 131 us; the launch traced here: 130 us
  Pallas kernels  102 us (78%)
  blocking collectives  10.8 us (8%)
  other arithmetic  8.58 us (7%)
  local copies, waits for them, and re-layouts  6.04 us (5%)
  matrix products  2.93 us (2%)
    pallas_call x1, Pallas kernels, body(): pl.pallas_call(exchange_kernel, in_specs=[smem, vmem, vmem], out_specs=[v...  76.7 us
    pallas_call x1, Pallas kernels, body(): pl.pallas_call(attend_kernel, grid_spec=pltpu.PrefetchScalarGridSpec(num_...  17.4 us
    all_to_all x1, blocking collectives, summed_on_arrival(): blocks = lax.all_to_all(split_up(x, dim, count), axis, 0, 0, tiled=True)  8.29 us
    pallas_call x1, Pallas kernels, body(): pl.pallas_call(project_kernel, grid=(tok_count // tile,), in_specs=[pl.Bl...  7.86 us
    convert_element_type x1, other arithmetic, body(): (projected * scale_rows[:, None] * norm_gain[None, :]).astype(jnp.bfloat16)  3.37 us
    dot_general x1, matrix products, body(): terms = jnp.dot(mixed_rows, out_weight, preferred_element_type=jnp.float32)  2.93 us

profile of v1, /device:TPU:1, one launch (start us, length us, event | category | flops | bytes accessed | tf_op | source)
XLA Modules:
  0.0 130.4 jit_solution(5254697426580355637)
XLA Ops:
  0.0 1.0 constant_dynamic-slice_fusion
  1.0 0.1 copy.31
  1.2 0.8 dynamic-slice_bitcast_fusion
  2.2 0.2 select_reduce_fusion
  2.3 0.7 reshape.122.t_ref
  3.1 0.1 dynamic_slice.16
  3.2 0.1 ne.69
  3.2 0.1 ge.10
  3.6 0.7 select_n.118.bias_ref
  4.3 0.5 fusion.8
  4.8 0.5 fusion.7.kidx_ref
  5.3 1.4 %fusion.2 = (f32[768,32]{1,0:T(8,128)S(1)}, f32[768,32]{1,0:T(8,128)S(1)}, f32[768,32]{1,0:T(8,128)S(1)}) fusion(f32[32]{0:T(128)S(1)} %multiply_power_fusion, f32[768]{0:T(1024)S(1)} %add_convert_fusion), kind=kLoop, calls=%fused_computation.13 | loop fusion | flops 49152 | bytes 298112 | tf_op jit(solution)/shard_map/neg | solution.py:238
  6.8 1.6 %pad_maximum_fusion = (f32[768,128]{1,0:T(8,128)}, f32[768,128]{1,0:T(8,128)}) fusion(f32[768,32]{1,0:T(8,128)S(1)} %get-tuple-element.22, f32[768,32]{1,0:T(8,128)S(1)} %get-tuple-element.21, f32[768,32]{1,0:T(8,128)S(1)} %get-tuple-element.20), kind=kLoop, calls=%fused_computation.9 | loop fusion | flops 589824 | bytes 1081344 | tf_op jit(solution)/shard_map/concatenate | solution.py:237
  8.3 7.9 %shard_map.82 = (bf16[768,512]{1,0:T(8,128)(2,1)}, bf16[768,128]{1,0:T(8,128)(2,1)}, bf16[768,128]{1,0:T(8,128)(2,1)}) custom-call(bf16[768,2048]{1,0:T(8,128)(2,1)} %bitcast.25, bf16[2048,512]{1,0:T(8,128)(2,1)} %wq_ref.1, bf16[2048,128]{1,0:T(8,128)(2,1)} %wk_ref.1, bf16[2048,128]{1,0:T(8,128)(2,1)} %wv_ref.1, f32[768,128]{1,0:T(8,128)} %get-tuple-element.27.cos_ref, ...), custom_call_target="tpu_custom_call" | custom-call | tf_op jit(solution)/shard_map/pallas_call | solution.py:240
  16.2 76.7 %shard_map.83 = (bf16[288,64,128]{2,1,0:T(8,128)(2,1)}, bf16[288,64,128]{2,1,0:T(8,128)(2,1)}) custom-call(s32[768]{0:T(1024)} %reshape.122.t_ref, bf16[12,64,128]{2,1,0:T(8,128)(2,1)} %bitcast.27, bf16[12,64,128]{2,1,0:T(8,128)(2,1)} %bitcast.28), custom_call_target="tpu_custom_call" | custom-call | tf_op jit(solution)/shard_map/pallas_call | solution.py:289
  92.9 17.4 %shard_map.84 = bf16[768,512]{1,0:T(8,128)(2,1)} custom-call(s32[96]{0:T(128)} %fusion.7.kidx_ref, s32[96]{0:T(128)} %get-tuple-element.17.vidx_ref, f32[6,1,1024]{2,1,0:T(1,128)} %select_n.118.bias_ref, bf16[768,512]{1,0:T(8,128)(2,1)} %get-tuple-element.10.q_ref, bf16[768,128]{1,0:T(8,128)(2,1)} %get-tuple-element.11.k_ref, ...), custom_call_target="tpu_custom_call" | custom-call | tf_op jit(solution)/shard_map/pallas_call | solution.py:307
  110.3 2.9 %convolution_convert_fusion = bf16[768,2048]{1,0:T(8,128)(2,1)S(1)} fusion(bf16[768,512]{1,0:T(8,128)(2,1)} %shard_map.84, bf16[512,2048]{1,0:T(8,128)(2,1)S(1)} %copy-done), kind=kOutput, calls=%fused_computation.1 | convolution fusion | flops 1612185600 | bytes 6029312 | tf_op jit(solution)/shard_map/dot_general | solution.py:331
  113.2 0.4 copy.34
  113.6 8.3 %all_to_all.5 = bf16[2,768,1024]{2,1,0:T(8,128)(2,1)S(1)} all-to-all(bf16[2,768,1024]{2,1,0:T(8,128)(2,1)S(1)} %bitcast.24), channel_id=1, replica_groups=mesh['dp'=4,'kv'=32,'tp'=2] {'tp'}, dimensions={0} | all-to-all | bytes 6291456 | tf_op jit(solution)/shard_map/all_to_all | solution.py:33
  121.9 0.7 convert_reduce_fusion
  122.6 1.7 %copy-done.1 = f32[768,1024]{1,0:T(8,128)} copy-done((f32[768,1024]{1,0:T(8,128)}, f32[768,1024]{1,0:T(8,128)S(1)}, u32[]{:S(2)}) %copy-start.1) | copy-done | bytes 3145752
  124.3 0.3 multiply_reduce_fusion
  124.5 2.5 %psum.7 = f32[768]{0:T(1024)S(1)} all-reduce(f32[768]{0:T(1024)S(1)} %multiply_reduce_fusion), channel_id=1, replica_groups=mesh['dp'=4,'kv'=32,'tp'=2] {'tp'}, use_global_device_ids=true, to_apply=%region_3.4 | all-reduce | flops 768 | bytes 6144 | tf_op jit(solution)/shard_map/psum | solution.py:333
  127.0 3.4 %fusion.1 = bf16[1,768,1024]{2,1,0:T(8,128)(2,1)} fusion(f32[768,1024]{1,0:T(8,128)} %copy-done.1, f32[1024]{0:T(1024)S(1)} %copy-done.2, f32[768]{0:T(1024)S(1)} %add_rsqrt_fusion), kind=kLoop, calls=%fused_computation.5 | loop fusion | flops 2359296 | bytes 4725760 | tf_op jit(solution)/shard_map/convert_element_type | solution.py:335
  (19 shorter events, 0.6 us)
Async XLA Ops:
  0.0 110.3 %copy-start = (bf16[512,2048]{1,0:T(8,128)(2,1)S(1)}, bf16[512,2048]{1,0:T(8,128)(2,1)}, u32[]{:S(2)}) copy-start(bf16[512,2048]{1,0:T(8,128)(2,1)} %param.12) | copy-start | bytes 6291460
  122.6 1.7 %copy-start.1 = (f32[768,1024]{1,0:T(8,128)}, f32[768,1024]{1,0:T(8,128)S(1)}, u32[]{:S(2)}) copy-start(f32[768,1024]{1,0:T(8,128)S(1)} %convert_reduce_fusion) | copy-start | bytes 9437188
  124.3 2.8 %copy-start.2 = (f32[1024]{0:T(1024)S(1)}, f32[1024]{0:T(1024)}, u32[]{:S(2)}) copy-start(f32[1024]{0:T(1024)} %param.13) | copy-start | bytes 12292

commit v2 on v0

v2 whole, which is shorter than its diff:
```python
import jax
import jax.numpy as jnp
from jax import lax
from jax.experimental import pallas as pl
from jax.experimental.pallas import tpu as pltpu
from jax.sharding import PartitionSpec as P

D = 2048
HEAD_DIM = 64
QUERY_BLOCK = 128
KEY_BLOCK = 64
NZ = 8
NX = 4
ROWS = 6
PARTS = 12
CHOSEN = 16
FULL = NZ * PARTS
SEL = NZ * ROWS
BLOCKS = 2 * FULL + 2 * SEL
rope_base = 10000.0
norm_eps = 1e-06
MESH = pl.DeviceIdType.MESH
LOG2E = 1.4426950408889634


def split_up(x, dim, count):
    before, after = (x.shape[:dim], x.shape[dim + 1 :])
    return jnp.moveaxis(x.reshape(*before, count, -1, *after), dim, 0)


def summed_on_arrival(x, axis, dim):
    count = lax.axis_size(axis)
    blocks = lax.all_to_all(split_up(x, dim, count), axis, 0, 0, tiled=True)
    return jnp.sum(blocks.astype(jnp.float32), axis=0)


def turned(u, cosine, sine, low_half):
    other = jnp.where(low_half, pltpu.roll(u, 96, 1), pltpu.roll(u, 32, 1))
    return u * cosine + other * sine


def project_kernel(z_ref, x_ref, wk_ref, wv_ref, cos_ref, sin_ref, owner_ref, part_ref, k_ref, v_ref, t_ref):
    x = x_ref[...]
    cosine, sine = cos_ref[...], sin_ref[...]
    lane = lax.broadcasted_iota(jnp.int32, cosine.shape, 1)
    low_half = (lane % HEAD_DIM) < HEAD_DIM // 2
    keys = jnp.dot(x, wk_ref[...], preferred_element_type=jnp.float32)
    k_ref[...] = turned(keys, cosine, sine, low_half).astype(jnp.bfloat16)
    v_ref[...] = jnp.dot(x, wv_ref[...], preferred_element_type=jnp.float32).astype(jnp.bfloat16)

    @pl.when(pl.program_id(0) == 0)
    def _():
        owner, part = owner_ref[...], part_ref[...]
        owner_at = lax.broadcasted_iota(jnp.int32, t_ref.shape, 1)
        table = jnp.full(t_ref.shape, -1, jnp.int32)
        for s in range(CHOSEN):
            table = jnp.where(owner[:, s : s + 1] == owner_at, part[:, s : s + 1], table)
        t_ref[...] = table


NEAR = (0, 1, 2, 6, 7)
FAR = (3, 4, 5)
WIDTH = 512
SUMS = 80


def exchange_kernel(
    t_ref, k_ref, v_ref, cos_ref, sin_ref, x_hbm, wq_hbm, out_ref,
    x_vm, wq_vm, qz, top_ref, acc_ref, whole,
    own_k, own_v, nb_k, nb_v,
    self_k, self_v, selfn_k, selfn_v,
    to_left_k, to_right_v, to_right_k, to_left_v, opp_k, opp_v, near_k, near_v,
    from_right_k, from_left_v, from_left_k, from_right_v, across_k, across_v, relay_k, relay_v,
    load_sem, zsend, zrecv, nsend, nrecv, ssend, srecv, rsend, rrecv,
):
    me = lax.axis_index("kv")
    z, x = me // NX, me % NX
    up = ((z + 1) % NZ) * NX + x
    down = ((z + NZ - 1) % NZ) * NX + x
    xr, xl, xo = (x + 1) % NX, (x + NX - 1) % NX, (x + 2) % NX
    right = z * NX + xr
    left = z * NX + xl
    load_x = pltpu.make_async_copy(x_hbm, x_vm, load_sem.at[0])
    load_w = pltpu.make_async_copy(wq_hbm, wq_vm, load_sem.at[1])
    load_x.start()
    load_w.start()
    barrier = pltpu.get_barrier_semaphore()
    for peer in (up, down, right, left):
        pl.semaphore_signal(barrier, inc=1, device_id={"kv": peer}, device_id_type=MESH)
    pl.semaphore_wait(barrier, 4)
    sent = []

    def send(src, dst, ssem, rsem, peer):
        copy = pltpu.make_async_remote_copy(
            src_ref=src, dst_ref=dst, send_sem=ssem, recv_sem=rsem,
            device_id={"kv": peer}, device_id_type=MESH,
        )
        copy.start()
        sent.append(copy)
        return copy

    def chunk(kind, slot):
        if kind < 2:
            if slot == 0:
                return (k_ref, v_ref)[kind]
            return (own_k, own_v)[kind].at[slot - 1]
        return (nb_k, nb_v)[kind - 2].at[NEAR.index(slot)]

    arrivals = {}

    def forward(kind, step):
        for direction in range(2):
            if step == NZ // 2 and kind % 2 != direction:
                continue
            new = step if direction == 0 else NZ - step
            old = (step - 1) if direction == 0 else (NZ - step + 1) % NZ
            arrivals[direction, step, kind] = send(
                chunk(kind, old), chunk(kind, new), zsend.at[direction, step - 1, kind],
                zrecv.at[direction, step - 1, kind], up if direction == 0 else down,
            )

    def owner_of(slot, column):
        return ((z + NZ - slot) % NZ) * NX + column

    def choose(target, dest_x, owner):
        for r in range(ROWS):
            part = t_ref[dest_x * ROWS + r, owner]
            target[r] = whole[jnp.maximum(part, 0)]

    got = {}

    def pick(kind, slot):
        is_v = kind % 2
        whole[...] = chunk(kind, slot)[...]
        jobs = []
        if kind < 2:
            owner = owner_of(slot, x)
            stage = (to_left_k, to_right_v)[is_v].at[slot]
            choose(stage, (xl, xr)[is_v], owner)
            jobs.append((stage, (from_right_k, from_left_v)[is_v].at[slot], 0, (left, right)[is_v]))
            if slot in FAR:
                at = FAR.index(slot)
                stage = (to_right_k, to_left_v)[is_v].at[at]
                choose(stage, (xr, xl)[is_v], owner)
                jobs.append((stage, (from_left_k, from_right_v)[is_v].at[at], 1, (right, left)[is_v]))
                stage = (opp_k, opp_v)[is_v].at[at]
                choose(stage, xo, owner)
                jobs.append((stage, (relay_k, relay_v)[is_v].at[at], 2, (right, left)[is_v]))
            choose((self_k, self_v)[is_v].at[slot], x, owner)
        else:
            owner = owner_of(slot, (xl, xr)[is_v])
            at = NEAR.index(slot)
            stage = (near_k, near_v)[is_v].at[at]
            choose(stage, (xr, xl)[is_v], owner)
            jobs.append((stage, (across_k, across_v)[is_v].at[slot], 3, (right, left)[is_v]))
            choose((selfn_k, selfn_v)[is_v].at[at], x, owner)
        for stage, place, which, peer in jobs:
            got[is_v, slot, which] = send(
                stage, place, ssend.at[is_v, slot, which], srecv.at[is_v, slot, which], peer)

    def pass_on(is_v, slot):
        at = FAR.index(slot)
        got[is_v, slot, 2].wait_recv()
        got[is_v, slot, 3] = send(
            (relay_k, relay_v)[is_v].at[at], (across_k, across_v)[is_v].at[slot],
            rsend.at[is_v, at], rrecv.at[is_v, at], (right, left)[is_v])

    def arrive(kind, step, onward):
        slots = []
        for direction in range(2):
            if (direction, step, kind) in arrivals:
                arrivals[direction, step, kind].wait_recv()
                slots.append(step if direction == 0 else NZ - step)
        if onward:
            forward(kind, step + 1)
        for slot in slots:
            pick(kind, slot)

    def candidate(slot, column):
        is_far = slot in FAR
        if column == "own":
            return self_k.at[slot], self_v.at[slot], owner_of(slot, x)
        if column == "right":
            values = from_right_v.at[FAR.index(slot)] if is_far else selfn_v.at[NEAR.index(slot)]
            return from_right_k.at[slot], values, owner_of(slot, xr)
        if column == "left":
            keys = from_left_k.at[FAR.index(slot)] if is_far else selfn_k.at[NEAR.index(slot)]
            return keys, from_left_v.at[slot], owner_of(slot, xl)
        return across_k.at[slot], across_v.at[slot], owner_of(slot, xo)

    def ready(slot):
        for is_v in range(2):
            got[is_v, slot, 0].wait_recv()
            if slot in FAR:
                got[is_v, slot, 1].wait_recv()
            got[is_v, slot, 3].wait_recv()

    scale = HEAD_DIM ** -0.5 * LOG2E

    def attend(names, first, last):
        blocks = [candidate(slot, column) for slot, column in names]

        def one_row(r, carry):
            keys = [b[0][r] for b in blocks]
            values = [b[1][r] for b in blocks]
            away = []
            for b in blocks:
                part = t_ref[x * ROWS + r, b[2]]
                away.append(jnp.where(part < 0, jnp.float32(jnp.inf), jnp.float32(0)))
            if first:
                for half in range(2):
                    keys.append(k_ref[2 * r + half])
                    values.append(v_ref[2 * r + half])
            all_keys = jnp.concatenate(keys, axis=0)
            turned_values = jnp.concatenate(values, axis=0).T
            far = len(blocks) * KEY_BLOCK
            count = all_keys.shape[0]
            ones = jnp.ones((SUMS - HEAD_DIM, count), jnp.bfloat16)
            for n in range(2):
                scores = lax.dot_general(
                    all_keys, qz[r, n], (((1,), (1,)), ((), ())), preferred_element_type=jnp.float32)
                pieces = [scores[KEY_BLOCK * i : KEY_BLOCK * (i + 1)] for i in range(len(blocks))]
                top = None if first else top_ref[r, n]
                old = top
                for piece, gone in zip(pieces, away):
                    peak = jnp.max(piece, axis=0, keepdims=True) - gone
                    top = peak if top is None else jnp.maximum(top, peak)
                if first:
                    key_at = lax.broadcasted_iota(jnp.int32, (QUERY_BLOCK, WIDTH), 0)
                    query_at = lax.broadcasted_iota(jnp.int32, (QUERY_BLOCK, WIDTH), 1) % QUERY_BLOCK
                    own = jnp.where(key_at <= query_at, scores[far:], -jnp.inf)
                    top = jnp.maximum(top, jnp.max(own, axis=0, keepdims=True))
                weights = [
                    jnp.exp2((piece - (top + gone)) * scale).astype(jnp.bfloat16)
                    for piece, gone in zip(pieces, away)
                ]
                if first:
                    weights.append(jnp.exp2((own - top) * scale).astype(jnp.bfloat16))
                left_side = jnp.concatenate(
                    [turned_values[HEAD_DIM * n : HEAD_DIM * (n + 1)], ones], axis=0)
                total = jnp.dot(
                    left_side, jnp.concatenate(weights, axis=0), preferred_element_type=jnp.float32)
                if not first:
                    total = total + acc_ref[r, n] * jnp.exp2((old - top) * scale)
                if not last:
                    top_ref[r, n] = top
                    acc_ref[r, n] = total
                else:
                    mixed = total[:HEAD_DIM] / total[HEAD_DIM : HEAD_DIM + 1]
                    at = pl.ds(pl.multiple_of(r * QUERY_BLOCK, QUERY_BLOCK), QUERY_BLOCK)
                    for p in range(2):
                        pair = jnp.concatenate(
                            [mixed[:, 256 * p : 256 * p + 128], mixed[:, 256 * p + 128 : 256 * p + 256]],
                            axis=0)
                        column = 256 * n + 128 * p
                        out_ref[at, column : column + 128] = pair.T.astype(jnp.bfloat16)
            return carry

        lax.fori_loop(0, ROWS, one_row, 0)

    def project_queries():
        load_x.wait()
        load_w.wait()

        def one_row(r, carry):
            at = pl.ds(pl.multiple_of(r * QUERY_BLOCK, QUERY_BLOCK), QUERY_BLOCK)
            q = jnp.dot(x_vm[at, :], wq_vm[...], preferred_element_type=jnp.float32)
            cosine, sine = cos_ref[at, :], sin_ref[at, :]
            lane = lax.broadcasted_iota(jnp.int32, cosine.shape, 1)
            low_half = (lane % HEAD_DIM) < HEAD_DIM // 2
            for n in range(2):
                mine = (lane < HEAD_DIM) if n == 0 else (lane >= HEAD_DIM)
                for p in range(2):
                    column = 256 * n + 128 * p
                    pair = turned(q[:, column : column + 128], cosine, sine, low_half)
                    other = pltpu.roll(pair, 64, 1)
                    for g in range(2):
                        head = pair if g == n else other
                        place = (2 * p + g) * QUERY_BLOCK
                        qz[r, n, place : place + QUERY_BLOCK] = jnp.where(mine, head, 0.0).astype(jnp.bfloat16)
            return carry

        lax.fori_loop(0, ROWS, one_row, 0)

    forward(0, 1)
    forward(1, 1)
    near0 = [
        send(k_ref, chunk(2, 0), nsend.at[0], nrecv.at[0], right),
        send(v_ref, chunk(3, 0), nsend.at[1], nrecv.at[1], left),
    ]
    pick(0, 0)
    pick(1, 0)
    project_queries()
    arrive(0, 1, True)
    for kind in (2, 3):
        near0[kind - 2].wait_recv()
        pick(kind, 0)
    arrive(1, 1, True)
    arrive(0, 2, True)
    ready(0)
    arrive(1, 2, True)
    attend([(0, c) for c in ("own", "right", "left", "across")], True, False)
    arrive(0, 3, True)
    arrive(1, 3, True)
    forward(2, 1)
    forward(3, 1)
    arrive(0, 4, False)
    pass_on(0, 3)
    pass_on(0, 5)
    arrive(1, 4, False)
    pass_on(1, 3)
    pass_on(1, 5)
    attend([(s, "own") for s in range(1, NZ)], False, False)
    arrive(2, 1, True)
    pass_on(0, 4)
    arrive(3, 1, True)
    pass_on(1, 4)
    for slot in FAR:
        ready(slot)
    attend([(s, c) for s in FAR for c in ("right", "left", "across")], False, False)
    arrive(2, 2, False)
    ready(1)
    ready(7)
    arrive(3, 2, False)
    attend([(s, c) for s in (1, 7) for c in ("right", "left", "across")], False, False)
    ready(2)
    ready(6)
    attend([(s, c) for s in (2, 6) for c in ("right", "left", "across")], False, True)
    for copy in sent:
        copy.wait_send()


def body(
    tokens, query_weight, key_weight, value_weight, out_weight, norm_gain, chosen_owner, chosen_part
):
    row_data = tokens[0]
    tok_count = row_data.shape[0]
    me = lax.axis_index("kv")
    z, x = me // NX, me % NX
    positions = me * tok_count + jnp.arange(tok_count, dtype=jnp.int32)
    half_dim = HEAD_DIM // 2
    lane = jnp.arange(128, dtype=jnp.int32)
    frequency = rope_base ** (-(lane % half_dim).astype(jnp.float32) / half_dim)
    angles = positions.astype(jnp.float32)[:, None] * frequency
    cosine = jnp.cos(angles)
    sine = jnp.sin(angles) * jnp.where(lane % HEAD_DIM < half_dim, -1.0, 1.0).astype(jnp.float32)
    tile = 256
    around = NX * ROWS
    keys, values, table = pl.pallas_call(
        project_kernel,
        grid_spec=pltpu.PrefetchScalarGridSpec(
            num_scalar_prefetch=1,
            grid=(tok_count // tile,),
            in_specs=[
                pl.BlockSpec((tile, D), lambda i, at: (i, 0)),
                pl.BlockSpec((D, 128), lambda i, at: (0, 0)),
                pl.BlockSpec((D, 128), lambda i, at: (0, 0)),
                pl.BlockSpec((tile, 128), lambda i, at: (i, 0)),
                pl.BlockSpec((tile, 128), lambda i, at: (i, 0)),
                pl.BlockSpec((around, CHOSEN), lambda i, at: (at[0], 0)),
                pl.BlockSpec((around, CHOSEN), lambda i, at: (at[0], 0)),
            ],
            out_specs=[
                pl.BlockSpec((tile, 128), lambda i, at: (i, 0)),
                pl.BlockSpec((tile, 128), lambda i, at: (i, 0)),
                pl.BlockSpec((around, NZ * NX), lambda i, at: (0, 0)),
            ],
        ),
        out_shape=[
            jax.ShapeDtypeStruct((tok_count, 128), jnp.bfloat16),
            jax.ShapeDtypeStruct((tok_count, 128), jnp.bfloat16),
            jax.ShapeDtypeStruct((around, NZ * NX), jnp.int32),
        ],
    )(z.reshape(1), row_data, key_weight, value_weight, cosine, sine, chosen_owner[0], chosen_part[0])

    vmem = pl.BlockSpec(memory_space=pltpu.VMEM)
    smem = pl.BlockSpec(memory_space=pltpu.SMEM)
    anyspace = pl.BlockSpec(memory_space=pl.ANY)

    def chunks(count):
        return pltpu.VMEM((count, PARTS, KEY_BLOCK, 128), jnp.bfloat16)

    def picks(count):
        return pltpu.VMEM((count, ROWS, KEY_BLOCK, 128), jnp.bfloat16)

    def sems(*shape):
        return pltpu.SemaphoreType.DMA(shape)

    mixed_rows = pl.pallas_call(
        exchange_kernel,
        in_specs=[smem, vmem, vmem, vmem, vmem, anyspace, anyspace],
        out_specs=vmem,
        out_shape=jax.ShapeDtypeStruct((tok_count, WIDTH), jnp.bfloat16),
        scratch_shapes=[
            pltpu.VMEM((tok_count, D), jnp.bfloat16),
            pltpu.VMEM((D, WIDTH), jnp.bfloat16),
            pltpu.VMEM((ROWS, 2, WIDTH, 128), jnp.bfloat16),
            pltpu.VMEM((ROWS, 2, 1, WIDTH), jnp.float32),
            pltpu.VMEM((ROWS, 2, SUMS, WIDTH), jnp.float32),
            pltpu.VMEM((PARTS, KEY_BLOCK, 128), jnp.bfloat16),
            chunks(7), chunks(7), chunks(5), chunks(5),
            picks(8), picks(8), picks(5), picks(5),
            picks(8), picks(8), picks(3), picks(3), picks(3), picks(3), picks(5), picks(5),
            picks(8), picks(8), picks(3), picks(3), picks(8), picks(8), picks(3), picks(3),
            sems(2),
            sems(2, 4, 4), sems(2, 4, 4),
            sems(2), sems(2),
            sems(2, 8, 4), sems(2, 8, 4),
            sems(2, 3), sems(2, 3),
        ],
        compiler_params=pltpu.CompilerParams(collective_id=0, has_side_effects=True),
    )(table, keys.reshape(PARTS, KEY_BLOCK, 128), values.reshape(PARTS, KEY_BLOCK, 128),
      cosine, sine, row_data, query_weight)

    terms = jnp.dot(mixed_rows, out_weight, preferred_element_type=jnp.float32)
    projected = summed_on_arrival(terms.astype(jnp.bfloat16), "tp", 1)
    row_total = lax.psum(jnp.sum(projected * projected, axis=1), "tp")
    scale_rows = lax.rsqrt(row_total / D + norm_eps)
    result = (projected * scale_rows[:, None] * norm_gain[None, :]).astype(jnp.bfloat16)
    return result[None]


def solution(mesh):
    placed = (
        P("dp", "kv", None),
        P(None, "tp"),
        P(None, "tp"),
        P(None, "tp"),
        P("tp", None),
        P("tp"),
        P("dp", None, None),
        P("dp", None, None),
    )
    return jax.shard_map(
        body, mesh=mesh, in_specs=placed, out_specs=P("dp", "kv", "tp"), check_vma=False
    )
```

time: 227 us -> 117 us (0.52)
  Pallas kernels: 0 us -> 90 us
  waiting for transfers between devices: 79.6 us -> 0 us
  local copies, waits for them, and re-layouts: 55.3 us -> 5.07 us
  matrix products: 51.1 us -> 2.93 us
  starting transfers between devices: 20.2 us -> 0 us
    pallas_call x0 -> x2, Pallas kernels: none -> 90 us  [the longest x1 84.6 us: body(): pl.pallas_call(exchange_kernel, in_specs=[smem, vmem, vmem, vmem, vmem, a...]
    all_to_all x2 -> x0, waiting for transfers between devices: 79.6 us -> none  [the longest x1 65.5 us: body(): lax.all_to_all(send_keys, 'kv', split_axis=0, concat_axis=0, tiled=True)]
    dot_general x5 -> x0, matrix products: 37.5 us -> none  [the longest x1 14.9 us: body(): jnp.einsum('bqngd,bknd->bngqk', block_queries, all_keys, preferred_elemen...]
    reshape x6 -> x0, local copies, waits for them, and re-layouts: 23.8 us -> none  [the longest x2 10.5 us: body(): picked_keys.reshape(qblocks, chosen_count * KEY_BLOCK, kv_here, HEAD_DIM)]
    all_to_all x2 -> x0, starting transfers between devices: 20.2 us -> none  [the longest x1 12 us: body(): lax.all_to_all(send_keys, 'kv', split_axis=0, concat_axis=0, tiled=True)]
    gather x4 -> x0, local copies, waits for them, and re-layouts: 13.2 us -> none  [the longest x1 3.83 us: body(): got_values.reshape(devices * qblocks, KEY_BLOCK, kv_width)[slot_index]]
    sub x1 -> x0, matrix products: 10.2 us -> none  [body(): weights = jnp.exp(scores - row_max)]
    unnamed x38 -> x8, local copies, waits for them, and re-layouts: 10.1 us -> 4.7 us
  transfers between devices with their start and end apart: 2 -> 0, of which waited for: 2 -> 0; matrix products, arithmetic and copies ran while one was open for 27% -> 0% of each run, Pallas kernels for 0% -> 0%
where the time goes in v2:
time: 117 us
  Pallas kernels  90 us (77%)
  blocking collectives  11.8 us (10%)
  other arithmetic  6.83 us (6%)
  local copies, waits for them, and re-layouts  5.07 us (4%)
  matrix products  2.93 us (3%)
    pallas_call x1, Pallas kernels, body(): pl.pallas_call(exchange_kernel, in_specs=[smem, vmem, vmem, vmem, vmem, a...  84.6 us
    all_to_all x1, blocking collectives, summed_on_arrival(): blocks = lax.all_to_all(split_up(x, dim, count), axis, 0, 0, tiled=True)  9.29 us
    pallas_call x1, Pallas kernels, body(): pl.pallas_call(project_kernel, grid_spec=pltpu.PrefetchScalarGridSpec(num...  5.44 us
    unnamed x8, local copies, waits for them, and re-layouts  4.7 us
    convert_element_type x1, other arithmetic, body(): (projected * scale_rows[:, None] * norm_gain[None, :]).astype(jnp.bfloat16)  3.37 us
    dot_general x1, matrix products, body(): terms = jnp.dot(mixed_rows, out_weight, preferred_element_type=jnp.float32)  2.93 us
    psum x1, blocking collectives, body(): row_total = lax.psum(jnp.sum(projected * projected, axis=1), 'tp')  2.5 us
    mul x1, other arithmetic, body(): jnp.sin(angles)  2.49 us

profile of v2, /device:TPU:1, one launch (start us, length us, event | category | flops | bytes accessed | tf_op | source)
XLA Modules:
  0.0 116.7 jit_solution(12168362440206707403)
XLA Ops:
  0.0 0.0 copy-start
  0.0 1.6 %copy.11 = s32[1,192,16]{2,1,0:T(8,128)} copy(s32[1,192,16]{1,2,0:T(8,128)} %param.14) | data formatting | bytes 24576 | tf_op args[6]
  1.6 1.4 %copy.12 = s32[1,192,16]{2,1,0:T(8,128)} copy(s32[1,192,16]{1,2,0:T(8,128)} %param.15) | data formatting | bytes 24576 | tf_op args[7]
  3.1 2.5 %fusion.2 = (f32[768,128]{1,0:T(8,128)}, f32[768,128]{1,0:T(8,128)}) fusion(f32[128]{0:T(128)S(1)} %get-tuple-element.13, f32[128]{0:T(128)S(1)} %get-tuple-element.14, f32[768]{0:T(1024)S(1)} %add_convert_fusion), kind=kLoop, calls=%fused_computation.9 | loop fusion | flops 196608 | bytes 790528 | tf_op jit(solution)/shard_map/mul | solution.py:346
  5.6 5.4 %shard_map.82 = (bf16[768,128]{1,0:T(8,128)(2,1)}, bf16[768,128]{1,0:T(8,128)(2,1)}, s32[24,32]{1,0:T(8,128)}) custom-call(s32[1]{0:T(128)} %bitcast.z_ref, bf16[768,2048]{1,0:T(8,128)(2,1)} %bitcast.22, bf16[2048,128]{1,0:T(8,128)(2,1)} %wk_ref.1, bf16[2048,128]{1,0:T(8,128)(2,1)} %wv_ref.1, f32[768,128]{1,0:T(8,128)} %get-tuple-element.12.cos_ref, ...), custom_call_target="tpu_custom_call" | custom-call | tf_op jit(solution)/shard_map/pallas_call | solution.py:349
  11.0 84.6 %shard_map.83 = bf16[768,512]{1,0:T(8,128)(2,1)} custom-call(s32[24,32]{1,0:T(8,128)} %get-tuple-element.8.t_ref, bf16[12,64,128]{2,1,0:T(8,128)(2,1)} %bitcast.27, bf16[12,64,128]{2,1,0:T(8,128)(2,1)} %bitcast.28, f32[768,128]{1,0:T(8,128)} %get-tuple-element.12.cos_ref, f32[768,128]{1,0:T(8,128)} %get-tuple-element.11.sin_ref, bf16[768,2048]{1,0:T(8,128)(2,1)} %bitcast.23, ...), custom_call_target="tpu_custom_call" | custom-call | tf_op jit(solution)/shard_map/pallas_call | solution.py:389
  95.6 0.0 copy-done
  95.6 2.9 %convolution_convert_fusion = bf16[768,2048]{1,0:T(8,128)(2,1)S(1)} fusion(bf16[768,512]{1,0:T(8,128)(2,1)} %shard_map.83, bf16[512,2048]{1,0:T(8,128)(2,1)S(1)} %copy-done), kind=kOutput, calls=%fused_computation.1 | convolution fusion | flops 1612185600 | bytes 6029312 | tf_op jit(solution)/shard_map/dot_general | solution.py:415
  98.6 0.4 copy.16
  98.9 9.3 %all_to_all.5 = bf16[2,768,1024]{2,1,0:T(8,128)(2,1)S(1)} all-to-all(bf16[2,768,1024]{2,1,0:T(8,128)(2,1)S(1)} %bitcast.21), channel_id=1, replica_groups=mesh['dp'=4,'kv'=32,'tp'=2] {'tp'}, dimensions={0} | all-to-all | bytes 6291456 | tf_op jit(solution)/shard_map/all_to_all | solution.py:33
  108.2 0.7 convert_reduce_fusion
  108.9 0.0 copy-start.1
  108.9 1.7 %copy-done.1 = f32[768,1024]{1,0:T(8,128)} copy-done((f32[768,1024]{1,0:T(8,128)}, f32[768,1024]{1,0:T(8,128)S(1)}, u32[]{:S(2)}) %copy-start.1) | copy-done | bytes 3145752
  110.6 0.0 copy-start.2
  110.6 0.3 multiply_reduce_fusion
  110.9 2.5 %psum.7 = f32[768]{0:T(1024)S(1)} all-reduce(f32[768]{0:T(1024)S(1)} %multiply_reduce_fusion), channel_id=1, replica_groups=mesh['dp'=4,'kv'=32,'tp'=2] {'tp'}, use_global_device_ids=true, to_apply=%region_2.3 | all-reduce | flops 768 | bytes 6144 | tf_op jit(solution)/shard_map/psum | solution.py:417
  113.4 0.0 copy-done.2
  113.4 3.4 %fusion.1 = bf16[1,768,1024]{2,1,0:T(8,128)(2,1)} fusion(f32[768,1024]{1,0:T(8,128)} %copy-done.1, f32[1024]{0:T(1024)S(1)} %copy-done.2, f32[768]{0:T(1024)S(1)} %add_rsqrt_fusion), kind=kLoop, calls=%fused_computation.5 | loop fusion | flops 2359296 | bytes 4725760 | tf_op jit(solution)/shard_map/convert_element_type | solution.py:419
  (3 shorter events, 0.0 us)
Async XLA Ops:
  0.0 95.6 %copy-start = (bf16[512,2048]{1,0:T(8,128)(2,1)S(1)}, bf16[512,2048]{1,0:T(8,128)(2,1)}, u32[]{:S(2)}) copy-start(bf16[512,2048]{1,0:T(8,128)(2,1)} %param.12) | copy-start | bytes 6291460
  108.9 1.7 %copy-start.1 = (f32[768,1024]{1,0:T(8,128)}, f32[768,1024]{1,0:T(8,128)S(1)}, u32[]{:S(2)}) copy-start(f32[768,1024]{1,0:T(8,128)S(1)} %convert_reduce_fusion) | copy-start | bytes 9437188
  110.6 2.8 %copy-start.2 = (f32[1024]{0:T(1024)S(1)}, f32[1024]{0:T(1024)}, u32[]{:S(2)}) copy-start(f32[1024]{0:T(1024)} %param.13) | copy-start | bytes 12292

commit v3 on v2

--- a/solution.py
+++ b/solution.py
@@ -39,7 +39,7 @@
     return u * cosine + other * sine
 
 
-def project_kernel(z_ref, x_ref, wk_ref, wv_ref, cos_ref, sin_ref, owner_ref, part_ref, k_ref, v_ref, t_ref):
+def project_kernel(x_ref, wk_ref, wv_ref, cos_ref, sin_ref, owner_ref, part_ref, k_ref, v_ref, t_ref):
     x = x_ref[...]
     cosine, sine = cos_ref[...], sin_ref[...]
     lane = lax.broadcasted_iota(jnp.int32, cosine.shape, 1)
@@ -51,15 +51,15 @@
     @pl.when(pl.program_id(0) == 0)
     def _():
         owner, part = owner_ref[...], part_ref[...]
-        owner_at = lax.broadcasted_iota(jnp.int32, t_ref.shape, 1)
+        owner_at = lax.broadcasted_iota(jnp.int32, t_ref.shape, 0)
         table = jnp.full(t_ref.shape, -1, jnp.int32)
         for s in range(CHOSEN):
-            table = jnp.where(owner[:, s : s + 1] == owner_at, part[:, s : s + 1], table)
+            table = jnp.where(owner[s : s + 1] == owner_at, part[s : s + 1], table)
         t_ref[...] = table
 
 
-NEAR = (0, 1, 2, 6, 7)
-FAR = (3, 4, 5)
+NEAR = ((0, 1, 2, 5, 6, 7), (0, 1, 2, 3, 6, 7))
+FAR = ((3, 4), (4, 5))
 WIDTH = 512
 SUMS = 80
 
@@ -104,13 +104,15 @@
             if slot == 0:
                 return (k_ref, v_ref)[kind]
             return (own_k, own_v)[kind].at[slot - 1]
-        return (nb_k, nb_v)[kind - 2].at[NEAR.index(slot)]
+        return (nb_k, nb_v)[kind - 2].at[NEAR[kind - 2].index(slot)]
 
     arrivals = {}
 
-    def forward(kind, step):
-        for direction in range(2):
+    def forward(kind, step, directions=(0, 1)):
+        for direction in directions:
             if step == NZ // 2 and kind % 2 != direction:
+                continue
+            if kind >= 2 and step == 3 and kind % 2 == direction:
                 continue
             new = step if direction == 0 else NZ - step
             old = (step - 1) if direction == 0 else (NZ - step + 1) % NZ
@@ -124,7 +126,7 @@
 
     def choose(target, dest_x, owner):
         for r in range(ROWS):
-            part = t_ref[dest_x * ROWS + r, owner]
+            part = t_ref[owner, (z * NX + dest_x) * ROWS + r]
             target[r] = whole[jnp.maximum(part, 0)]
 
     got = {}
@@ -138,8 +140,8 @@
             stage = (to_left_k, to_right_v)[is_v].at[slot]
             choose(stage, (xl, xr)[is_v], owner)
             jobs.append((stage, (from_right_k, from_left_v)[is_v].at[slot], 0, (left, right)[is_v]))
-            if slot in FAR:
-                at = FAR.index(slot)
+            if slot in FAR[is_v]:
+                at = FAR[is_v].index(slot)
                 stage = (to_right_k, to_left_v)[is_v].at[at]
                 choose(stage, (xr, xl)[is_v], owner)
                 jobs.append((stage, (from_left_k, from_right_v)[is_v].at[at], 1, (right, left)[is_v]))
@@ -149,7 +151,7 @@
             choose((self_k, self_v)[is_v].at[slot], x, owner)
         else:
             owner = owner_of(slot, (xl, xr)[is_v])
-            at = NEAR.index(slot)
+            at = NEAR[is_v].index(slot)
             stage = (near_k, near_v)[is_v].at[at]
             choose(stage, (xr, xl)[is_v], owner)
             jobs.append((stage, (across_k, across_v)[is_v].at[slot], 3, (right, left)[is_v]))
@@ -159,45 +161,58 @@
                 stage, place, ssend.at[is_v, slot, which], srecv.at[is_v, slot, which], peer)
 
     def pass_on(is_v, slot):
-        at = FAR.index(slot)
+        at = FAR[is_v].index(slot)
         got[is_v, slot, 2].wait_recv()
         got[is_v, slot, 3] = send(
             (relay_k, relay_v)[is_v].at[at], (across_k, across_v)[is_v].at[slot],
             rsend.at[is_v, at], rrecv.at[is_v, at], (right, left)[is_v])
 
-    def arrive(kind, step, onward):
+    def arrive(kind, step, onward, directions=(0, 1)):
         slots = []
-        for direction in range(2):
+        for direction in directions:
             if (direction, step, kind) in arrivals:
                 arrivals[direction, step, kind].wait_recv()
                 slots.append(step if direction == 0 else NZ - step)
-        if onward:
-            forward(kind, step + 1)
+                if onward:
+                    forward(kind, step + 1, (direction,))
         for slot in slots:
             pick(kind, slot)
 
     def candidate(slot, column):
-        is_far = slot in FAR
         if column == "own":
             return self_k.at[slot], self_v.at[slot], owner_of(slot, x)
         if column == "right":
-            values = from_right_v.at[FAR.index(slot)] if is_far else selfn_v.at[NEAR.index(slot)]
+            values = (
+                from_right_v.at[FAR[1].index(slot)] if slot in FAR[1] else selfn_v.at[NEAR[1].index(slot)])
             return from_right_k.at[slot], values, owner_of(slot, xr)
         if column == "left":
-            keys = from_left_k.at[FAR.index(slot)] if is_far else selfn_k.at[NEAR.index(slot)]
+            keys = from_left_k.at[FAR[0].index(slot)] if slot in FAR[0] else selfn_k.at[NEAR[0].index(slot)]
             return keys, from_left_v.at[slot], owner_of(slot, xl)
         return across_k.at[slot], across_v.at[slot], owner_of(slot, xo)
 
-    def ready(slot):
-        for is_v in range(2):
-            got[is_v, slot, 0].wait_recv()
-            if slot in FAR:
-                got[is_v, slot, 1].wait_recv()
-            got[is_v, slot, 3].wait_recv()
+    waited = set()
+
+    def ready(names):
+        for slot, column in names:
+            if column == "own":
+                continue
+            for is_v in range(2):
+                if column == "across":
+                    which = 3
+                elif (column == "right") == (is_v == 0):
+                    which = 0
+                elif slot in FAR[is_v]:
+                    which = 1
+                else:
+                    continue
+                if (is_v, slot, which) not in waited:
+                    waited.add((is_v, slot, which))
+                    got[is_v, slot, which].wait_recv()
 
     scale = HEAD_DIM ** -0.5 * LOG2E
 
     def attend(names, first, last):
+        ready(names)
         blocks = [candidate(slot, column) for slot, column in names]
 
         def one_row(r, carry):
@@ -205,7 +220,7 @@
             values = [b[1][r] for b in blocks]
             away = []
             for b in blocks:
-                part = t_ref[x * ROWS + r, b[2]]
+                part = t_ref[b[2], me * ROWS + r]
                 away.append(jnp.where(part < 0, jnp.float32(jnp.inf), jnp.float32(0)))
             if first:
                 for half in range(2):
@@ -217,8 +232,7 @@
             count = all_keys.shape[0]
             ones = jnp.ones((SUMS - HEAD_DIM, count), jnp.bfloat16)
             for n in range(2):
-                scores = lax.dot_general(
-                    all_keys, qz[r, n], (((1,), (1,)), ((), ())), preferred_element_type=jnp.float32)
+                scores = jnp.dot(all_keys, qz[r, n], preferred_element_type=jnp.float32)
                 pieces = [scores[KEY_BLOCK * i : KEY_BLOCK * (i + 1)] for i in range(len(blocks))]
                 top = None if first else top_ref[r, n]
                 old = top
@@ -256,7 +270,7 @@
                         out_ref[at, column : column + 128] = pair.T.astype(jnp.bfloat16)
             return carry
 
-        lax.fori_loop(0, ROWS, one_row, 0)
+        lax.fori_loop(0, ROWS, one_row, 0, unroll=2)
 
     def project_queries():
         load_x.wait()
@@ -269,19 +283,20 @@
             lane = lax.broadcasted_iota(jnp.int32, cosine.shape, 1)
             low_half = (lane % HEAD_DIM) < HEAD_DIM // 2
             for n in range(2):
-                mine = (lane < HEAD_DIM) if n == 0 else (lane >= HEAD_DIM)
                 for p in range(2):
                     column = 256 * n + 128 * p
-                    pair = turned(q[:, column : column + 128], cosine, sine, low_half)
-                    other = pltpu.roll(pair, 64, 1)
+                    pair = turned(q[:, column : column + 128], cosine, sine, low_half).T.astype(jnp.bfloat16)
                     for g in range(2):
-                        head = pair if g == n else other
+                        head = pair[HEAD_DIM * g : HEAD_DIM * (g + 1)]
                         place = (2 * p + g) * QUERY_BLOCK
-                        qz[r, n, place : place + QUERY_BLOCK] = jnp.where(mine, head, 0.0).astype(jnp.bfloat16)
+                        qz[r, n, HEAD_DIM * n : HEAD_DIM * (n + 1), place : place + QUERY_BLOCK] = head
+                        qz[r, n, HEAD_DIM * (1 - n) : HEAD_DIM * (2 - n), place : place + QUERY_BLOCK] = (
+                            jnp.zeros_like(head))
             return carry
 
         lax.fori_loop(0, ROWS, one_row, 0)
 
+    others = ("right", "left", "across")
     forward(0, 1)
     forward(1, 1)
     near0 = [
@@ -296,36 +311,38 @@
         near0[kind - 2].wait_recv()
         pick(kind, 0)
     arrive(1, 1, True)
+    attend([(0, c) for c in ("own",) + others], True, False)
     arrive(0, 2, True)
-    ready(0)
     arrive(1, 2, True)
-    attend([(0, c) for c in ("own", "right", "left", "across")], True, False)
+    attend([(s, "own") for s in (1, 7, 2, 6)], False, False)
     arrive(0, 3, True)
+    forward(3, 1, (0,))
+    forward(2, 1, (1,))
     arrive(1, 3, True)
-    forward(2, 1)
-    forward(3, 1)
+    forward(2, 1, (0,))
+    forward(3, 1, (1,))
+    attend([(3, "own"), (5, "own")], False, False)
     arrive(0, 4, False)
+    arrive(3, 1, True, (0,))
+    arrive(2, 1, True, (1,))
     pass_on(0, 3)
-    pass_on(0, 5)
     arrive(1, 4, False)
-    pass_on(1, 3)
     pass_on(1, 5)
-    attend([(s, "own") for s in range(1, NZ)], False, False)
-    arrive(2, 1, True)
+    attend([(4, "own"), (3, "left"), (5, "right")], False, False)
+    arrive(2, 1, True, (0,))
+    arrive(3, 1, True, (1,))
     pass_on(0, 4)
-    arrive(3, 1, True)
     pass_on(1, 4)
-    for slot in FAR:
-        ready(slot)
-    attend([(s, c) for s in FAR for c in ("right", "left", "across")], False, False)
-    arrive(2, 2, False)
-    ready(1)
-    ready(7)
-    arrive(3, 2, False)
-    attend([(s, c) for s in (1, 7) for c in ("right", "left", "across")], False, False)
-    ready(2)
-    ready(6)
-    attend([(s, c) for s in (2, 6) for c in ("right", "left", "across")], False, True)
+    arrive(3, 2, True, (0,))
+    arrive(2, 2, True, (1,))
+    attend([(4, c) for c in others], False, False)
+    arrive(2, 2, False, (0,))
+    arrive(3, 2, False, (1,))
+    attend([(s, c) for s in (1, 7) for c in others], False, False)
+    arrive(3, 3, False, (0,))
+    arrive(2, 3, False, (1,))
+    attend([(s, c) for s in (2, 6) for c in others], False, False)
+    attend([(3, "right"), (3, "across"), (5, "left"), (5, "across")], False, True)
     for copy in sent:
         copy.wait_send()
 
@@ -345,33 +362,32 @@
     cosine = jnp.cos(angles)
     sine = jnp.sin(angles) * jnp.where(lane % HEAD_DIM < half_dim, -1.0, 1.0).astype(jnp.float32)
     tile = 256
-    around = NX * ROWS
+    qblocks = chosen_owner.shape[1]
     keys, values, table = pl.pallas_call(
         project_kernel,
-        grid_spec=pltpu.PrefetchScalarGridSpec(
-            num_scalar_prefetch=1,
+        grid_spec=pl.GridSpec(
             grid=(tok_count // tile,),
             in_specs=[
-                pl.BlockSpec((tile, D), lambda i, at: (i, 0)),
-                pl.BlockSpec((D, 128), lambda i, at: (0, 0)),
-                pl.BlockSpec((D, 128), lambda i, at: (0, 0)),
-                pl.BlockSpec((tile, 128), lambda i, at: (i, 0)),
-                pl.BlockSpec((tile, 128), lambda i, at: (i, 0)),
-                pl.BlockSpec((around, CHOSEN), lambda i, at: (at[0], 0)),
-                pl.BlockSpec((around, CHOSEN), lambda i, at: (at[0], 0)),
+                pl.BlockSpec((tile, D), lambda i: (i, 0)),
+                pl.BlockSpec((D, 128), lambda i: (0, 0)),
+                pl.BlockSpec((D, 128), lambda i: (0, 0)),
+                pl.BlockSpec((tile, 128), lambda i: (i, 0)),
+                pl.BlockSpec((tile, 128), lambda i: (i, 0)),
+                pl.BlockSpec((CHOSEN, qblocks), lambda i: (0, 0)),
+                pl.BlockSpec((CHOSEN, qblocks), lambda i: (0, 0)),
             ],
             out_specs=[
-                pl.BlockSpec((tile, 128), lambda i, at: (i, 0)),
-                pl.BlockSpec((tile, 128), lambda i, at: (i, 0)),
-                pl.BlockSpec((around, NZ * NX), lambda i, at: (0, 0)),
+                pl.BlockSpec((tile, 128), lambda i: (i, 0)),
+                pl.BlockSpec((tile, 128), lambda i: (i, 0)),
+                pl.BlockSpec((NZ * NX, qblocks), lambda i: (0, 0)),
             ],
         ),
         out_shape=[
             jax.ShapeDtypeStruct((tok_count, 128), jnp.bfloat16),
             jax.ShapeDtypeStruct((tok_count, 128), jnp.bfloat16),
-            jax.ShapeDtypeStruct((around, NZ * NX), jnp.int32),
+            jax.ShapeDtypeStruct((NZ * NX, qblocks), jnp.int32),
         ],
-    )(z.reshape(1), row_data, key_weight, value_weight, cosine, sine, chosen_owner[0], chosen_part[0])
+    )(row_data, key_weight, value_weight, cosine, sine, chosen_owner[0].T, chosen_part[0].T)
 
     vmem = pl.BlockSpec(memory_space=pltpu.VMEM)
     smem = pl.BlockSpec(memory_space=pltpu.SMEM)
@@ -394,19 +410,19 @@
         scratch_shapes=[
             pltpu.VMEM((tok_count, D), jnp.bfloat16),
             pltpu.VMEM((D, WIDTH), jnp.bfloat16),
-            pltpu.VMEM((ROWS, 2, WIDTH, 128), jnp.bfloat16),
+            pltpu.VMEM((ROWS, 2, 128, WIDTH), jnp.bfloat16),
             pltpu.VMEM((ROWS, 2, 1, WIDTH), jnp.float32),
             pltpu.VMEM((ROWS, 2, SUMS, WIDTH), jnp.float32),
             pltpu.VMEM((PARTS, KEY_BLOCK, 128), jnp.bfloat16),
-            chunks(7), chunks(7), chunks(5), chunks(5),
-            picks(8), picks(8), picks(5), picks(5),
-            picks(8), picks(8), picks(3), picks(3), picks(3), picks(3), picks(5), picks(5),
-            picks(8), picks(8), picks(3), picks(3), picks(8), picks(8), picks(3), picks(3),
+            chunks(7), chunks(7), chunks(6), chunks(6),
+            picks(8), picks(8), picks(6), picks(6),
+            picks(8), picks(8), picks(2), picks(2), picks(2), picks(2), picks(6), picks(6),
+            picks(8), picks(8), picks(2), picks(2), picks(8), picks(8), picks(2), picks(2),
             sems(2),
             sems(2, 4, 4), sems(2, 4, 4),
             sems(2), sems(2),
             sems(2, 8, 4), sems(2, 8, 4),
-            sems(2, 3), sems(2, 3),
+            sems(2, 2), sems(2, 2),
         ],
         compiler_params=pltpu.CompilerParams(collective_id=0, has_side_effects=True),
     )(table, keys.reshape(PARTS, KEY_BLOCK, 128), values.reshape(PARTS, KEY_BLOCK, 128),

time: 117 us -> 109 us (0.932)
  Pallas kernels: 90 us -> 84.2 us
  local copies, waits for them, and re-layouts: 5.07 us -> 2.03 us
  blocking collectives: 11.8 us -> 13.1 us
    pallas_call x1, Pallas kernels: 84.6 us -> 79 us  [body(): pl.pallas_call(exchange_kernel, in_specs=[smem, vmem, vmem, vmem, vmem, a...]
    unnamed x8 -> x6, local copies, waits for them, and re-layouts: 4.7 us -> 1.67 us
    all_to_all x1, blocking collectives: 9.29 us -> 10.6 us  [summed_on_arrival(): blocks = lax.all_to_all(split_up(x, dim, count), axis, 0, 0, tiled=True)]
where the time goes in v3:
time: 109 us
  Pallas kernels  84.2 us (77%)
  blocking collectives  13.1 us (12%)
  other arithmetic  6.86 us (6%)
  matrix products  2.93 us (3%)
  local copies, waits for them, and re-layouts  2.03 us (2%)
    pallas_call x1, Pallas kernels, body(): pl.pallas_call(exchange_kernel, in_specs=[smem, vmem, vmem, vmem, vmem, a...  79 us
    all_to_all x1, blocking collectives, summed_on_arrival(): blocks = lax.all_to_all(split_up(x, dim, count), axis, 0, 0, tiled=True)  10.6 us
    pallas_call x1, Pallas kernels, body(): pl.pallas_call(project_kernel, grid_spec=pl.GridSpec(grid=(tok_count // t...  5.18 us
    convert_element_type x1, other arithmetic, body(): (projected * scale_rows[:, None] * norm_gain[None, :]).astype(jnp.bfloat16)  3.37 us
    dot_general x1, matrix products, body(): terms = jnp.dot(mixed_rows, out_weight, preferred_element_type=jnp.float32)  2.93 us
    mul x1, other arithmetic, body(): jnp.sin(angles)  2.51 us
    psum x1, blocking collectives, body(): row_total = lax.psum(jnp.sum(projected * projected, axis=1), 'tp')  2.5 us

profile of v3, /device:TPU:1, one launch (start us, length us, event | category | flops | bytes accessed | tf_op | source)
XLA Modules:
  0.0 109.2 jit_solution(16401292431410794769)
XLA Ops:
  0.0 0.0 copy-start
  0.0 2.5 %fusion.2 = (f32[768,128]{1,0:T(8,128)}, f32[768,128]{1,0:T(8,128)}) fusion(f32[128]{0:T(128)S(1)} %get-tuple-element.13, f32[128]{0:T(128)S(1)} %get-tuple-element.14, f32[768]{0:T(1024)S(1)} %add_convert_fusion), kind=kLoop, calls=%fused_computation.9 | loop fusion | flops 196608 | bytes 790528 | tf_op jit(solution)/shard_map/mul | solution.py:363
  2.5 5.2 %shard_map.82 = (bf16[768,128]{1,0:T(8,128)(2,1)}, bf16[768,128]{1,0:T(8,128)(2,1)}, s32[32,192]{1,0:T(8,128)}) custom-call(bf16[768,2048]{1,0:T(8,128)(2,1)} %bitcast.24, bf16[2048,128]{1,0:T(8,128)(2,1)} %wk_ref.1, bf16[2048,128]{1,0:T(8,128)(2,1)} %wv_ref.1, f32[768,128]{1,0:T(8,128)} %get-tuple-element.12.cos_ref, f32[768,128]{1,0:T(8,128)} %get-tuple-element.11.sin_ref, ...), custom_call_target="tpu_custom_call" | custom-call | tf_op jit(solution)/shard_map/pallas_call | solution.py:366
  7.7 79.0 %shard_map.83 = bf16[768,512]{1,0:T(8,128)(2,1)} custom-call(s32[32,192]{1,0:T(8,128)} %get-tuple-element.8.t_ref, bf16[12,64,128]{2,1,0:T(8,128)(2,1)} %bitcast.28, bf16[12,64,128]{2,1,0:T(8,128)(2,1)} %bitcast.29, f32[768,128]{1,0:T(8,128)} %get-tuple-element.12.cos_ref, f32[768,128]{1,0:T(8,128)} %get-tuple-element.11.sin_ref, ...), custom_call_target="tpu_custom_call" | custom-call | tf_op jit(solution)/shard_map/pallas_call | solution.py:405
  86.7 0.0 copy-done
  86.8 2.9 %convolution_convert_fusion = bf16[768,2048]{1,0:T(8,128)(2,1)S(1)} fusion(bf16[768,512]{1,0:T(8,128)(2,1)} %shard_map.83, bf16[512,2048]{1,0:T(8,128)(2,1)S(1)} %copy-done), kind=kOutput, calls=%fused_computation.1 | convolution fusion | flops 1612185600 | bytes 6029312 | tf_op jit(solution)/shard_map/dot_general | solution.py:431
  89.7 0.4 copy.12
  90.1 10.6 %all_to_all.5 = bf16[2,768,1024]{2,1,0:T(8,128)(2,1)S(1)} all-to-all(bf16[2,768,1024]{2,1,0:T(8,128)(2,1)S(1)} %bitcast.26), channel_id=1, replica_groups=mesh['dp'=4,'kv'=32,'tp'=2] {'tp'}, dimensions={0} | all-to-all | bytes 6291456 | tf_op jit(solution)/shard_map/all_to_all | solution.py:33
  100.7 0.7 convert_reduce_fusion
  101.3 0.0 copy-start.1
  101.4 1.7 %copy-done.1 = f32[768,1024]{1,0:T(8,128)} copy-done((f32[768,1024]{1,0:T(8,128)}, f32[768,1024]{1,0:T(8,128)S(1)}, u32[]{:S(2)}) %copy-start.1) | copy-done | bytes 3145752
  103.0 0.0 copy-start.2
  103.0 0.3 multiply_reduce_fusion
  103.3 2.5 %psum.7 = f32[768]{0:T(1024)S(1)} all-reduce(f32[768]{0:T(1024)S(1)} %multiply_reduce_fusion), channel_id=1, replica_groups=mesh['dp'=4,'kv'=32,'tp'=2] {'tp'}, use_global_device_ids=true, to_apply=%region_2.3 | all-reduce | flops 768 | bytes 6144 | tf_op jit(solution)/shard_map/psum | solution.py:433
  105.8 0.0 copy-done.2
  105.8 3.4 %fusion.1 = bf16[1,768,1024]{2,1,0:T(8,128)(2,1)} fusion(f32[768,1024]{1,0:T(8,128)} %copy-done.1, f32[1024]{0:T(1024)S(1)} %copy-done.2, f32[768]{0:T(1024)S(1)} %add_rsqrt_fusion), kind=kLoop, calls=%fused_computation.5 | loop fusion | flops 2359296 | bytes 4725760 | tf_op jit(solution)/shard_map/convert_element_type | solution.py:435
  (3 shorter events, 0.0 us)
Async XLA Ops:
  0.0 86.7 %copy-start = (bf16[512,2048]{1,0:T(8,128)(2,1)S(1)}, bf16[512,2048]{1,0:T(8,128)(2,1)}, u32[]{:S(2)}) copy-start(bf16[512,2048]{1,0:T(8,128)(2,1)} %param.12) | copy-start | bytes 6291460
  101.3 1.7 %copy-start.1 = (f32[768,1024]{1,0:T(8,128)}, f32[768,1024]{1,0:T(8,128)S(1)}, u32[]{:S(2)}) copy-start(f32[768,1024]{1,0:T(8,128)S(1)} %convert_reduce_fusion) | copy-start | bytes 9437188
  103.0 2.8 %copy-start.2 = (f32[1024]{0:T(1024)S(1)}, f32[1024]{0:T(1024)}, u32[]{:S(2)}) copy-start(f32[1024]{0:T(1024)} %param.13) | copy-start | bytes 12292
